TPU v7x, 32 devices: a whole 2x2x4 slice. The times are simulated.
32 devices in a mesh: ep: 8 (over z, x), tp: 4 (over y, core).
Axes of the slice: x: 2, y: 2, z: 4, core: 2. Of those that a mesh axis runs over, the one named last changes fastest.
Arguments:
- projected_queries: bfloat16 [2048, 2048], P('ep', 'tp'), may hold values from -245 to 245, as said below
- key_proj: bfloat16 [2048, 512], P('ep', 'tp'), may hold values from -6.2 to 6.2
- projected_values: bfloat16 [2048, 512], P('ep', 'tp'), may hold values from -24 to 24
- head_sink_logits: float32 [32], P('tp'), may hold values from 1 to 6
- out_weight: bfloat16 [2048, 4096], P('tp'), may hold values from -0.125 to 0.125
- expert_input: bfloat16 [1024, 4096], P('ep'), may hold values from -6 to 6
- norm_gain: float32 [4096], replicated, may hold values from 0.1 to 1.9
- routing: int32 [1024, 4], P('ep'), may hold values from 0 to 7, all different within a row; in each aligned block of 128 rows (0 to 127, 128 to 255, ...) at most 96 rows name the same one
- route_weight: float32 [1024, 4], P('ep'), may hold values from 0.1 to 1
- gate_weight: bfloat16 [8, 4096, 1024], P('ep', None, 'tp'), may hold values from -0.27929688 to 0.27929688
- up_weight: bfloat16 [8, 4096, 1024], P('ep', None, 'tp'), may hold values from -0.27929688 to 0.27929688
- down_weight: bfloat16 [8, 1024, 4096], P('ep', 'tp'), may hold values from -0.046875 to 0.046875
Outputs:
- mixer_output: bfloat16 [2048, 4096], P(('ep', 'tp'))
- expert_output: bfloat16 [1024, 4096], P('ep', 'tp')
Inputs may be any that keep to these rules, and one draw needn't show every extreme that they name: `projected_queries`: in the hidden draw some queries nearly equal a large multiple of a nearby key. `routing`: each row names 4 different experts; among the rows of one device (aligned blocks of 128 rows) no expert is named more than 96 times, a bound that some block reaches.
All inputs are finite; a program needn't handle non-finite values.
Results may differ from a plain program's by a relative error of at most 0.014.
Values may be sent and summed in bfloat16 or wider, within the bound.
A program may use at most 128 MiB of HBM per device.

v0:
```python
import jax
import jax.numpy as jnp
from jax import lax
from jax.experimental import pallas as pl
from jax.experimental.pallas import tpu as pltpu
from jax.sharding import PartitionSpec as P

D = 4096
HEAD_SIZE = 64
WINDOW_KEYS = 128
TOPK = 4


EPS = 1e-06
CLAMP = 7.0
SLOPE = 1.702


def passed_along(block, axis, distance):
    devices = range(lax.axis_size(axis))
    route = [(i - distance, i) for i in devices if i - distance in devices]
    return lax.ppermute(block, axis, route)


LINE = 4
MESH = pl.DeviceIdType.MESH


def chosen(z, values):
    result = jnp.int32(values[0])
    for place in range(1, LINE):
        result = jnp.where(z == place, jnp.int32(values[place]), result)
    return result


def nearest_first(place):
    return sorted(range(LINE), key=lambda other: (abs(other - place), other))


def layer_kernel(
    token_ref,
    gain_ref,
    share_ref,
    gate_hbm,
    up_hbm,
    down_hbm,
    query_ref,
    key_ref,
    value_ref,
    sink_ref,
    project_hbm,
    mixer_ref,
    out_ref,
    own_ref,
    gate_ref,
    up_ref,
    down_ref,
    project_ref,
    halo_ref,
    attended_ref,
    mixed_ref,
    mixed_core_ref,
    mixed_pair_ref,
    load_sem,
    halo_send,
    halo_recv,
    mixed_core_send,
    mixed_core_recv,
    mixed_pair_send,
    mixed_pair_recv,
    rows_ref,
    weight_ref,
    sum_ref,
    core_ref,
    pair_ref,
    side_ref,
    up_line_ref,
    down_line_ref,
    last_ref,
    share_send,
    share_recv,
    line_send,
    line_recv,
    side_send,
    side_recv,
    pair_send,
    pair_recv,
    core_send,
    core_recv,
    back_core_send,
    back_core_recv,
    back_pair_send,
    back_pair_recv,
    back_side_send,
    back_side_recv,
    back_line_send,
    back_line_recv,
    last_send,
    last_recv,
):
    e, t = lax.axis_index("ep"), lax.axis_index("tp")
    z, x, y, c = e // 2, e % 2, t // 2, t % 2
    tokens, width = token_ref.shape
    sibling, partner, beside = (e, y * 2 + 1 - c), (e, (1 - y) * 2 + c), (z * 2 + 1 - x, t)
    above, below = (e + 2, t), (e - 2, t)

    def copy(src, dst, send, recv, to):
        return pltpu.make_async_remote_copy(
            src_ref=src, dst_ref=dst, send_sem=send, recv_sem=recv, device_id=to, device_id_type=MESH
        )

    loads = [
        pltpu.make_async_copy(src, dst, load_sem.at[place])
        for place, (src, dst) in enumerate(
            [(project_hbm, project_ref), (gate_hbm, gate_ref), (up_hbm, up_ref), (down_hbm, down_ref)]
        )
    ]
    for load in loads:
        load.start()
    barrier = pltpu.get_barrier_semaphore()
    for step in range(1, 2 * LINE):
        pl.semaphore_signal(
            barrier, inc=1, device_id=((e + step) % (2 * LINE), t), device_id_type=MESH
        )
    for other in (sibling, partner):
        pl.semaphore_signal(barrier, inc=1, device_id=other, device_id_type=MESH)
    widened = token_ref[...].astype(jnp.float32)
    scale = lax.rsqrt(jnp.mean(widened * widened, axis=-1, keepdims=True) + EPS)
    own_ref[...] = (widened * scale * gain_ref[...]).astype(jnp.bfloat16)
    rows_ref[e] = own_ref[...]
    pl.semaphore_wait(barrier, 2 * LINE + 1)

    lone = width * 3 // 16
    both = width // 8
    first = pl.multiple_of(y * (width - 2 * lone) + c * lone, 128)
    middle = pl.multiple_of(2 * lone + c * both, 128)
    other_first = pl.multiple_of((1 - y) * (width - 2 * lone) + c * lone, 128)
    parts = (pl.ds(first, lone), pl.ds(middle, both), pl.ds(other_first, lone))

    def view(block, part):
        return rows_ref.at[block, :, parts[part]]

    def source(block, part, mine):
        return own_ref.at[:, parts[part]] if mine else view(block, part)

    def along(way, at, part, mine, to):
        block = at * 2 + x
        return copy(
            source(block, part, mine), view(block, part),
            line_send.at[way, at, part], line_recv.at[at, part], to,
        )

    def across(at, part, mine):
        block = at * 2 + x
        return copy(
            source(block, part, mine), view(block, part),
            side_send.at[at, part], side_recv.at[at, part], beside,
        )

    def across_in(at, part):
        block = at * 2 + 1 - x
        return copy(
            view(block, part), view(block, part), side_send.at[at, part], side_recv.at[at, part], beside
        )

    def to_partner(block):
        return copy(view(block, 0), view(block, 0), pair_send.at[block], pair_recv.at[block], partner)

    def from_partner(block):
        return copy(view(block, 2), view(block, 2), pair_send.at[block], pair_recv.at[block], partner)

    def to_sibling(block, part):
        return copy(
            view(block, part), view(block, part), core_send.at[block, part], core_recv.at[block, part], sibling
        )

    sibling_parts = (
        pl.ds(pl.multiple_of(y * (width - 2 * lone) + (1 - c) * lone, 128), lone),
        pl.ds(pl.multiple_of(2 * lone + (1 - c) * both, 128), both),
        pl.ds(pl.multiple_of((1 - y) * (width - 2 * lone) + (1 - c) * lone, 128), lone),
    )

    def from_sibling(block, part):
        dst = rows_ref.at[block, :, sibling_parts[part]]
        return copy(dst, dst, core_send.at[block, part], core_recv.at[block, part], sibling)

    def share_copy(step):
        to = (e + step) % (2 * LINE)
        return copy(
            share_ref.at[to], weight_ref.at[e], share_send.at[step], share_recv.at[e], (to, t)
        )

    def share_in(step):
        at = (e + step) % (2 * LINE)
        return copy(share_ref.at[at], weight_ref.at[at], share_send.at[step], share_recv.at[at], (at, t))

    for part in (0, 1):
        @pl.when(z < LINE - 1)
        def _():
            along(0, z, part, True, above).start()

        @pl.when(z > 0)
        def _():
            along(1, z, part, True, below).start()

        across(z, part, True).start()
    queries = query_ref.shape[0]

    def halo_copy(which):
        src = (key_ref, value_ref)[which].at[pl.ds(queries - WINDOW_KEYS, WINDOW_KEYS)]
        to = ((e + 1) % (2 * LINE), t)
        return copy(src, halo_ref.at[which], halo_send.at[which], halo_recv.at[which], to)

    @pl.when(e < 2 * LINE - 1)
    def _():
        halo_copy(0).start()
        halo_copy(1).start()

    @pl.when(e == 0)
    def _():
        halo_ref[...] = jnp.zeros_like(halo_ref)

    for step in range(1, 2 * LINE):
        share_copy(step).start()
    weight_ref[e] = share_ref[e]

    kv_heads = key_ref.shape[1] // HEAD_SIZE
    group = query_ref.shape[1] // HEAD_SIZE // kv_heads
    span = queries // 4
    here = lax.broadcasted_iota(jnp.int32, (WINDOW_KEYS, 2 * WINDOW_KEYS), 0)
    there = lax.broadcasted_iota(jnp.int32, (WINDOW_KEYS, 2 * WINDOW_KEYS), 1)

    def attend(number):
        begin = number * WINDOW_KEYS
        permitted = (there > here) & (there <= here + WINDOW_KEYS)
        if number == 0:
            permitted = permitted & ((there >= WINDOW_KEYS) | (e > 0))
        for kv in range(kv_heads):
            lanes = slice(kv * HEAD_SIZE, (kv + 1) * HEAD_SIZE)
            if number == 0:
                keys = jnp.concatenate([halo_ref[0][:, lanes], key_ref[0:WINDOW_KEYS, lanes]], axis=0)
                values = jnp.concatenate(
                    [halo_ref[1][:, lanes], value_ref[0:WINDOW_KEYS, lanes]], axis=0
                )
            else:
                keys = key_ref[begin - WINDOW_KEYS : begin + WINDOW_KEYS, lanes]
                values = value_ref[begin - WINDOW_KEYS : begin + WINDOW_KEYS, lanes]
            for member in range(group):
                head = kv * group + member
                columns = slice(head * HEAD_SIZE, (head + 1) * HEAD_SIZE)
                scores = lax.dot_general(
                    query_ref[begin : begin + WINDOW_KEYS, columns],
                    keys,
                    (((1,), (1,)), ((), ())),
                    preferred_element_type=jnp.float32,
                ) * HEAD_SIZE ** (-0.5)
                scores = jnp.where(permitted, scores, -jnp.inf)
                sink = sink_ref[head]
                highest = jnp.maximum(jnp.max(scores, axis=-1, keepdims=True), sink)
                numerator = jnp.exp(scores - highest)
                denominator = jnp.sum(numerator, axis=-1, keepdims=True) + jnp.exp(sink - highest)
                weights = (numerator / denominator).astype(jnp.bfloat16)
                found = jnp.dot(weights, values, preferred_element_type=jnp.float32)
                attended_ref[begin : begin + WINDOW_KEYS, columns] = found.astype(jnp.bfloat16)

    def mixed_core(half):
        at = pl.multiple_of((half * 2 + 1 - c) * span, 16)
        return copy(
            mixed_ref.at[pl.ds(at, span)], mixed_core_ref.at[half],
            mixed_core_send.at[half], mixed_core_recv.at[half], sibling,
        )

    mixed_pair = copy(
        mixed_ref.at[pl.ds(pl.multiple_of(((1 - y) * 2 + c) * span, 16), span)], mixed_pair_ref,
        mixed_pair_send, mixed_pair_recv, partner,
    )

    def mixed_rows(half):
        return pl.ds(pl.multiple_of((half * 2 + c) * span, 16), span)

    def mix():
        for number in range(1, queries // WINDOW_KEYS):
            attend(number)

        @pl.when(e > 0)
        def _():
            halo_copy(0).wait_recv()
            halo_copy(1).wait_recv()

        attend(0)
        loads[0].wait()
        for place in range(0, width, width // 4):
            columns = slice(place, place + width // 4)
            mixed_ref[:, columns] = jnp.dot(
                attended_ref[...], project_ref[:, columns], preferred_element_type=jnp.float32
            ).astype(jnp.bfloat16)
        for half in range(2):
            mixed_core(half).start()

    def mix_onward():
        for half in range(2):
            mixed_core(half).wait_recv()
            total = mixed_ref[mixed_rows(half), :].astype(jnp.float32)
            mixed_ref[mixed_rows(half), :] = (
                total + mixed_core_ref[half].astype(jnp.float32)
            ).astype(jnp.bfloat16)

    mix()
    near = [chosen(z, [nearest_first(place)[j] for place in range(LINE)]) for j in range(LINE)]
    sequence = []

    def passed_on(block):
        to_partner(block).start()
        to_sibling(block, 0).start()
        to_sibling(block, 1).start()
        sequence.append(block)

    def settle(block):
        from_partner(block).wait_recv()
        to_sibling(block, 2).start()

    for j in range(1, LINE + 1):
        if j < LINE:
            at = near[j]
            for part in (0, 1):
                along(0, at, part, False, above).wait_recv()

                @pl.when((at < z) & (z < LINE - 1))
                def _():
                    along(0, at, part, False, above).start()

                @pl.when((at > z) & (z > 0))
                def _():
                    along(1, at, part, False, below).start()

                across(at, part, False).start()
            passed_on(at * 2 + x)
            if len(sequence) > 2:
                settle(sequence[len(sequence) - 3])
        for part in (0, 1):
            across_in(near[j - 1], part).wait_recv()
        passed_on(near[j - 1] * 2 + 1 - x)
        if len(sequence) > 2:
            settle(sequence[len(sequence) - 3])
    mix_onward()
    for block in sequence[-2:]:
        settle(block)
    for load in loads[1:]:
        load.wait()
    for step in range(1, 2 * LINE):
        share_in(step).wait_recv()
    for block in sequence:
        for part in range(3):
            from_sibling(block, part).wait_recv()

    quarter = width // 4
    early = quarter * 5 // 8
    late = quarter - early
    mine = pl.multiple_of((y * 2 + c) * quarter, 128)
    theirs = pl.multiple_of(((1 - y) * 2 + c) * quarter, 128)
    early_mine, early_theirs = pl.ds(mine, early), pl.ds(theirs, early)
    late_mine = pl.ds(pl.multiple_of(mine + early, 128), late)
    late_theirs = pl.ds(pl.multiple_of(theirs + early, 128), late)
    own_quarter, other_quarter = pl.ds(mine, quarter), pl.ds(theirs, quarter)
    sent_quarters = [
        pl.ds(pl.multiple_of((half * 2 + 1 - c) * quarter, 128), quarter) for half in range(2)
    ]
    kept_quarters = [
        pl.ds(pl.multiple_of((half * 2 + c) * quarter, 128), quarter) for half in range(2)
    ]
    trio = ((early_mine, 0, early), (late_mine, early, late), (late_theirs, quarter, late))

    def add(block, columns, arrived):
        total = sum_ref[block, :, columns].astype(jnp.float32)
        sum_ref[block, :, columns] = (total + arrived.astype(jnp.float32)).astype(jnp.bfloat16)

    def far(j):
        result = chosen(z, [nearest_first(place)[::-1][0] for place in range(LINE)])
        for index in range(1, LINE):
            value = chosen(z, [nearest_first(place)[::-1][index] for place in range(LINE)])
            result = jnp.where(j == index, value, result)
        return result

    def back_core(block, half, columns):
        return copy(
            sum_ref.at[block, :, columns], core_ref.at[block, :, pl.ds(half * quarter, quarter)],
            back_core_send.at[block, half], back_core_recv.at[block, half], sibling,
        )

    def back_pair(block):
        return copy(
            sum_ref.at[block, :, early_theirs], pair_ref.at[block],
            back_pair_send.at[block], back_pair_recv.at[block], partner,
        )

    def back_side(at, index):
        columns, start, length = trio[index]
        return copy(
            sum_ref.at[at * 2 + 1 - x, :, columns], side_ref.at[at, :, pl.ds(start, length)],
            back_side_send.at[at, index], back_side_recv.at[at, index], beside,
        )

    def back_line(way, at, index, to):
        columns, start, length = trio[index]
        landing = (up_line_ref, down_line_ref)[way]
        return copy(
            sum_ref.at[at * 2 + x, :, columns], landing.at[at, :, pl.ds(start, length)],
            back_line_send.at[at, index], back_line_recv.at[way, at, index], to,
        )

    def line_in(way, at):
        for index, (columns, start, length) in enumerate(trio):
            back_line(way, at, index, above).wait_recv()
            landing = (up_line_ref, down_line_ref)[way]
            add(at * 2 + x, columns, landing[at, :, start : start + length])

    last = copy(sum_ref.at[e, :, late_theirs], last_ref, last_send, last_recv, partner)

    def experts_of(block):
        rows = rows_ref[block]
        gate_pre = jnp.dot(rows, gate_ref[...], preferred_element_type=jnp.float32)
        up_pre = jnp.dot(rows, up_ref[...], preferred_element_type=jnp.float32)
        gate_cut = jnp.minimum(gate_pre, CLAMP)
        activated = (
            (jnp.clip(up_pre, -CLAMP, CLAMP) + 1.0) * gate_cut * jax.nn.sigmoid(SLOPE * gate_cut)
        ).astype(jnp.bfloat16)
        weight = jnp.broadcast_to(weight_ref[block][0:1], (tokens, tokens)).T[:, 0:1]

        for place in range(0, width, quarter):
            result = jnp.dot(
                activated, down_ref[:, place : place + quarter], preferred_element_type=jnp.float32
            )
            sum_ref[block, :, place : place + quarter] = (result * weight).astype(jnp.bfloat16)

    def turn(i, carry):
        @pl.when(i < LINE)
        def _():
            at = far(i)

            def one(index, inner):
                block = at * 2 + (1 - x) * (1 - index) + x * index
                experts_of(block)
                for half in range(2):
                    back_core(block, half, sent_quarters[half]).start()
                return inner

            lax.fori_loop(0, 2, one, 0)

        @pl.when((i >= 1) & (i < LINE + 1))
        def _():
            at = far(i - 1)

            def one(index, inner):
                block = at * 2 + (1 - x) * (1 - index) + x * index
                for half in range(2):
                    back_core(block, half, sent_quarters[half]).wait_recv()
                    add(block, kept_quarters[half], core_ref[block, :, half * quarter : (half + 1) * quarter])
                back_pair(block).start()
                return inner

            lax.fori_loop(0, 2, one, 0)

        @pl.when(i == LINE)
        def _():
            mixed_pair.start()

        @pl.when((i >= 2) & (i < LINE + 2))
        def _():
            at = far(i - 2)

            def one(index, inner):
                block = at * 2 + (1 - x) * (1 - index) + x * index
                back_pair(block).wait_recv()
                add(block, early_mine, pair_ref[block])

                @pl.when(index == 0)
                def _():
                    for part in range(3):
                        back_side(at, part).start()

                return inner

            lax.fori_loop(0, 2, one, 0)

        @pl.when(i >= 3)
        def _():
            at = far(i - 3)
            for part, (columns, start, length) in enumerate(trio):
                back_side(at, part).wait_recv()
                add(at * 2 + x, columns, side_ref[at, :, start : start + length])

            @pl.when((at >= z) & (z > 0))
            def _():
                line_in(0, at)

            @pl.when((at <= z) & (z < LINE - 1))
            def _():
                line_in(1, at)

            @pl.when(at > z)
            def _():
                for part in range(3):
                    back_line(0, at, part, above).start()

            @pl.when(at < z)
            def _():
                for part in range(3):
                    back_line(1, at, part, below).start()

        return carry

    lax.fori_loop(0, LINE + 3, turn, 0)
    last.start()
    last.wait_recv()
    out_ref[:, 0:early] = sum_ref[e, :, early_mine]
    closing = sum_ref[e, :, late_mine].astype(jnp.float32) + last_ref[...].astype(jnp.float32)
    out_ref[:, early:quarter] = closing.astype(jnp.bfloat16)

    mixed_pair.wait_recv()
    total = mixed_ref[mixed_rows(y), :].astype(jnp.float32)
    mixer_ref[...] = (total + mixed_pair_ref[...].astype(jnp.float32)).astype(jnp.bfloat16)

    last.wait_send()
    mixed_pair.wait_send()
    for half in range(2):
        mixed_core(half).wait_send()

    @pl.when(e < 2 * LINE - 1)
    def _():
        halo_copy(0).wait_send()
        halo_copy(1).wait_send()

    for part in (0, 1):
        @pl.when(z < LINE - 1)
        def _():
            along(0, z, part, True, above).wait_send()

        @pl.when(z > 0)
        def _():
            along(1, z, part, True, below).wait_send()

        across(z, part, True).wait_send()
    for step in range(1, 2 * LINE):
        share_copy(step).wait_send()
    for j in range(1, LINE):
        at = near[j]
        for part in (0, 1):
            @pl.when((at < z) & (z < LINE - 1))
            def _():
                along(0, at, part, False, above).wait_send()

            @pl.when((at > z) & (z > 0))
            def _():
                along(1, at, part, False, below).wait_send()

            across(at, part, False).wait_send()
    for block in sequence:
        to_partner(block).wait_send()
        for part in range(3):
            to_sibling(block, part).wait_send()

    def drained(at, carry):
        for side in range(2):
            for half in range(2):
                back_core(at * 2 + side, half, sent_quarters[half]).wait_send()
            back_pair(at * 2 + side).wait_send()
        for part in range(3):
            back_side(at, part).wait_send()

            @pl.when(at != z)
            def _():
                back_line(0, at, part, above).wait_send()

        return carry

    lax.fori_loop(0, LINE, drained, 0)


def layer_call(
    rows, gain, share_of, gate_one, up_one, down_one, queries, keys, values, sinks, project
):
    tokens, width = rows.shape
    quarter = width // 4
    early = quarter * 5 // 8
    carried = quarter + quarter - early
    blocks = 2 * LINE
    kept = jnp.bfloat16
    dma = pltpu.SemaphoreType.DMA
    span = queries.shape[0] // 4
    in_vmem = pl.BlockSpec(memory_space=pltpu.VMEM)
    in_smem = pl.BlockSpec(memory_space=pltpu.SMEM)
    stays = pl.BlockSpec(memory_space=pl.ANY)
    return pl.pallas_call(
        layer_kernel,
        out_shape=(
            jax.ShapeDtypeStruct((span, width), kept),
            jax.ShapeDtypeStruct((tokens, quarter), kept),
        ),
        in_specs=[in_vmem] * 3 + [stays] * 3 + [in_vmem] * 3 + [in_smem, stays],
        out_specs=(in_vmem, in_vmem),
        scratch_shapes=[
            pltpu.VMEM(rows.shape, kept),
            pltpu.VMEM(gate_one.shape, kept),
            pltpu.VMEM(up_one.shape, kept),
            pltpu.VMEM(down_one.shape, kept),
            pltpu.VMEM(project.shape, kept),
            pltpu.VMEM((2, WINDOW_KEYS, keys.shape[1]), kept),
            pltpu.VMEM(queries.shape, kept),
            pltpu.VMEM((queries.shape[0], width), kept),
            pltpu.VMEM((2, span, width), kept),
            pltpu.VMEM((span, width), kept),
            dma((4,)),
            dma((2,)),
            dma((2,)),
            dma((2,)),
            dma((2,)),
            dma,
            dma,
            pltpu.VMEM((blocks, tokens, width), kept),
            pltpu.VMEM((blocks, 8, tokens), jnp.float32),
            pltpu.VMEM((blocks, tokens, width), kept),
            pltpu.VMEM((blocks, tokens, 2 * quarter), kept),
            pltpu.VMEM((blocks, tokens, early), kept),
            pltpu.VMEM((LINE, tokens, carried), kept),
            pltpu.VMEM((LINE, tokens, carried), kept),
            pltpu.VMEM((LINE, tokens, carried), kept),
            pltpu.VMEM((tokens, quarter - early), kept),
            dma((blocks,)),
            dma((blocks,)),
            dma((2, LINE, 2)),
            dma((LINE, 2)),
            dma((LINE, 2)),
            dma((LINE, 2)),
            dma((blocks,)),
            dma((blocks,)),
            dma((blocks, 3)),
            dma((blocks, 3)),
            dma((blocks, 2)),
            dma((blocks, 2)),
            dma((blocks,)),
            dma((blocks,)),
            dma((LINE, 3)),
            dma((LINE, 3)),
            dma((LINE, 3)),
            dma((2, LINE, 3)),
            dma,
            dma,
        ],
        compiler_params=pltpu.CompilerParams(
            collective_id=0, has_side_effects=True, vmem_limit_bytes=60 * 1024 * 1024
        ),
        cost_estimate=pl.CostEstimate(
            flops=8 * blocks * tokens * width * gate_one.shape[1],
            bytes_accessed=8 * width * gate_one.shape[1],
            transcendentals=0,
        ),
    )(rows, gain, share_of, gate_one, up_one, down_one, queries, keys, values, sinks, project)


def shards(
    projected_queries,
    key_proj,
    projected_values,
    head_sink_logits,
    out_weight,
    expert_input,
    norm_gain,
    routing,
    route_weight,
    gate_weight,
    up_weight,
    down_weight,
):
    token_rows = expert_input.shape[0]
    experts = lax.axis_size("ep")
    capacity = max(3 * token_rows * TOPK // (2 * experts), 2)
    col_share = D // lax.axis_size("tp")
    widened = expert_input.astype(jnp.float32)
    normed = (
        widened
        * lax.rsqrt(jnp.mean(widened * widened, axis=-1, keepdims=True) + EPS)
        * norm_gain[None, :]
    ).astype(jnp.bfloat16)
    if (experts, lax.axis_size("tp")) == (2 * LINE, 4) and token_rows == 128:
        named = routing == lax.broadcasted_iota(jnp.int32, (experts, 1, 1), 0)
        share_of = jnp.sum(jnp.where(named, route_weight[None], 0.0), axis=2)
        share_of = jnp.broadcast_to(share_of[:, None, :], (experts, 8, token_rows))
        return layer_call(
            expert_input,
            norm_gain[None, :],
            share_of,
            gate_weight[0],
            up_weight[0],
            down_weight[0],
            projected_queries,
            key_proj,
            projected_values,
            head_sink_logits,
            out_weight,
        )
    query_rows = projected_queries.shape[0]
    kv_heads = key_proj.shape[1] // HEAD_SIZE
    heads_per_group = projected_queries.shape[1] // HEAD_SIZE // kv_heads
    count_of_blocks = query_rows // WINDOW_KEYS
    prior_key, prior_value = passed_along(
        (key_proj[query_rows - WINDOW_KEYS :], projected_values[query_rows - WINDOW_KEYS :]),
        "ep",
        1,
    )
    key_all = jnp.concatenate([prior_key, key_proj], axis=0)
    value_all = jnp.concatenate([prior_value, projected_values], axis=0)
    window_keys = jnp.concatenate(
        [
            key_all[:-WINDOW_KEYS].reshape(count_of_blocks, WINDOW_KEYS, kv_heads, HEAD_SIZE),
            key_all[WINDOW_KEYS:].reshape(count_of_blocks, WINDOW_KEYS, kv_heads, HEAD_SIZE),
        ],
        axis=1,
    )
    window_values = jnp.concatenate(
        [
            value_all[:-WINDOW_KEYS].reshape(count_of_blocks, WINDOW_KEYS, kv_heads, HEAD_SIZE),
            value_all[WINDOW_KEYS:].reshape(count_of_blocks, WINDOW_KEYS, kv_heads, HEAD_SIZE),
        ],
        axis=1,
    )
    query_blocks = projected_queries.reshape(
        count_of_blocks, WINDOW_KEYS, kv_heads, heads_per_group, HEAD_SIZE
    )
    scores = jnp.einsum(
        "nqhgd,nshd->nhgqs", query_blocks, window_keys, preferred_element_type=jnp.float32
    ) * HEAD_SIZE ** (-0.5)
    offset = lax.axis_index("ep") * query_rows
    block_ids = jnp.arange(count_of_blocks)[:, None, None] * WINDOW_KEYS + offset
    query_pos = block_ids + jnp.arange(WINDOW_KEYS)[None, :, None]
    key_pos = block_ids - WINDOW_KEYS + jnp.arange(2 * WINDOW_KEYS)[None, None, :]
    permitted_mask = (key_pos <= query_pos) & (query_pos - key_pos < WINDOW_KEYS) & (key_pos >= 0)
    scores = jnp.where(permitted_mask[:, None, None, :, :], scores, -jnp.inf)
    sink_col = head_sink_logits.reshape(kv_heads, heads_per_group)[None, :, :, None, None]
    highest = jnp.maximum(jnp.max(scores, axis=-1, keepdims=True), sink_col)
    numerator = jnp.exp(scores - highest)
    denominator = jnp.sum(numerator, axis=-1, keepdims=True) + jnp.exp(sink_col - highest)
    weights = (numerator / denominator).astype(jnp.bfloat16)
    attended = jnp.einsum(
        "nhgqs,nshd->nqhgd", weights, window_values, preferred_element_type=jnp.float32
    )
    attended = attended.astype(jnp.bfloat16).reshape(
        query_rows, kv_heads * heads_per_group * HEAD_SIZE
    )
    mixer_output = lax.psum_scatter(
        jnp.dot(attended, out_weight, preferred_element_type=jnp.float32).astype(jnp.bfloat16),
        "tp",
        scatter_dimension=0,
        tiled=True,
    )
    flat_ids = routing.reshape(-1)
    onehot = (flat_ids[:, None] == jnp.arange(experts, dtype=jnp.int32)[None, :]).astype(jnp.int32)
    rank_in = jnp.cumsum(onehot, axis=0) - 1
    target = flat_ids * capacity + jnp.sum(rank_in * onehot, axis=1)
    tok_ids = jnp.arange(token_rows * TOPK) // TOPK
    slot_tok = jnp.full((experts * capacity,), token_rows, jnp.int32).at[target].set(tok_ids)
    gate_one = gate_weight[0]
    up_one = up_weight[0]
    own_cols = lax.dynamic_slice_in_dim(normed, lax.axis_index("tp") * col_share, col_share, 1)
    extended = jnp.concatenate([own_cols, jnp.zeros((1, col_share), jnp.bfloat16)], axis=0)
    outgoing = jnp.take(extended, slot_tok, axis=0).reshape(experts, capacity, col_share)
    arrived = lax.all_to_all(outgoing, "ep", split_axis=0, concat_axis=0, tiled=True).reshape(
        experts * capacity, col_share
    )
    portion = lax.all_gather(arrived, "tp", axis=1, tiled=True)
    gate_pre = jnp.dot(portion, gate_one, preferred_element_type=jnp.float32)
    up_pre = jnp.dot(portion, up_one, preferred_element_type=jnp.float32)
    gate_cut = jnp.minimum(gate_pre, CLAMP)
    activated = (
        (jnp.clip(up_pre, -CLAMP, CLAMP) + 1.0) * gate_cut * jax.nn.sigmoid(SLOPE * gate_cut)
    ).astype(jnp.bfloat16)
    partial_value = jnp.dot(activated, down_weight[0], preferred_element_type=jnp.float32)
    expert_result = lax.psum_scatter(
        partial_value.astype(jnp.bfloat16), "tp", scatter_dimension=1, tiled=True
    )
    returned = lax.all_to_all(
        expert_result.reshape(experts, capacity, col_share),
        "ep",
        split_axis=0,
        concat_axis=0,
        tiled=True,
    )
    picked = jnp.take(returned.reshape(experts * capacity, col_share), target, axis=0)
    picked = picked.astype(jnp.float32).reshape(token_rows, TOPK, col_share)
    expert_output = jnp.sum(picked * route_weight[:, :, None], axis=1).astype(jnp.bfloat16)
    return (mixer_output, expert_output)


def solution(mesh):
    placed = (
        P("ep", "tp"),
        P("ep", "tp"),
        P("ep", "tp"),
        P("tp"),
        P("tp", None),
        P("ep", None),
        P(),
        P("ep", None),
        P("ep", None),
        P("ep", None, "tp"),
        P("ep", None, "tp"),
        P("ep", "tp", None),
    )
    return jax.shard_map(
        shards,
        mesh=mesh,
        in_specs=placed,
        out_specs=(P(("ep", "tp"), None), P("ep", "tp")),
        check_vma=False,
    )
```

profile of v0, /device:TPU:0, one launch (start us, length us, event | category | flops | bytes accessed | tf_op | source)
XLA Modules:
  0.0 114.0 jit_solution(18118232150314239206)
XLA Ops:
  0.6 0.7 select_reduce_fusion
  1.3 0.6 broadcast_in_dim.26.share_ref
  2.0 108.5 %shard_map.131 = (bf16[64,4096]{1,0:T(8,128)(2,1)}, bf16[128,1024]{1,0:T(8,128)(2,1)}) custom-call(bf16[128,4096]{1,0:T(8,128)(2,1)} %token_ref.1, f32[1,4096]{1,0:T(1,128)} %bitcast.7, f32[8,8,128]{2,1,0:T(8,128)} %broadcast_in_dim.26.share_ref, bf16[4096,256]{1,0:T(8,128)(2,1)} %bitcast.4, bf16[4096,256]{1,0:T(8,128)(2,1)} %bitcast.5, ...), custom_call_target="tpu_custom_call" | custom-call | flops 8589934592 | bytes 8388608 | tf_op jit(solution)/shard_map/pallas_call | solution.py:593
  110.4 1.9 %copy.18 = bf16[64,4096]{1,0:T(8,128)(2,1)} copy(bf16[64,4096]{1,0:T(8,128)(2,1)} %get-tuple-element.4) | data formatting | bytes 1048576
  112.3 1.7 %copy.19 = bf16[128,1024]{1,0:T(8,128)(2,1)} copy(bf16[128,1024]{1,0:T(8,128)(2,1)} %get-tuple-element.5) | data formatting | bytes 524288
where the time goes:
time: 114 us
  Pallas kernels  108 us (95%)
  local copies, waits for them, and re-layouts  4.16 us (4%)
    pallas_call x1, Pallas kernels, layer_call(): pl.pallas_call(layer_kernel, out_shape=(jax.ShapeDtypeStruct((span, width...  108 us
    unnamed x2, local copies, waits for them, and re-layouts  3.54 us

commit v1 on v0

v1 whole, which is shorter than its diff:
```python
import types

import jax
import jax.numpy as jnp
from jax import lax
from jax.experimental import pallas as pl
from jax.experimental.pallas import tpu as pltpu
from jax.sharding import PartitionSpec as P

D = 4096
HEAD_SIZE = 64
WINDOW_KEYS = 128
TOPK = 4


EPS = 1e-06
CLAMP = 7.0
SLOPE = 1.702


def passed_along(block, axis, distance):
    devices = range(lax.axis_size(axis))
    route = [(i - distance, i) for i in devices if i - distance in devices]
    return lax.ppermute(block, axis, route)


LINE = 4
SLOTS = 96
LONE = 4
EARLY = 5
MIXED_CUTS = 4
MESH = pl.DeviceIdType.MESH

NAMES = (
    "token_hbm", "gain_hbm", "routing_hbm", "route_weight_hbm", "query_hbm", "key_hbm",
    "value_hbm", "sink_hbm", "project_hbm", "gate_hbm", "up_hbm", "down_hbm", "mixer", "out",
    "token", "gain", "routing", "route_weight", "query", "key", "value", "sink", "own", "dense",
    "packed", "aside", "both_weights", "down", "project", "halo", "attended", "mixed",
    "mixed_core", "mixed_pair", "shares", "ranks", "hot", "slot_weight", "active", "results",
    "pair", "side", "line_out", "line_in", "last", "final", "mixer_kept", "out_kept", "keep_sem", "load_sem", "halo_send", "halo_recv",
    "mixed_core_send", "mixed_core_recv", "mixed_pair_send", "mixed_pair_recv", "share_send",
    "share_recv", "own_send", "onward_send", "along_recv", "across_send", "across_recv",
    "partner_send", "partner_recv", "core_send", "core_recv", "down_send", "down_recv",
    "active_send", "active_recv", "pair_send", "pair_recv", "side_send", "side_recv", "line_send",
    "line_recv", "last_send", "last_recv",
)


def chosen(z, values):
    result = jnp.int32(values[0])
    for place in range(1, LINE):
        result = jnp.where(z == place, jnp.int32(values[place]), result)
    return result


def nearest_first(place):
    return sorted(range(LINE), key=lambda other: (abs(other - place), abs(2 * other - LINE + 1)))


def sizes_of(width):
    quarter = width // 4
    lone = width * LONE // 32
    both = (width - 4 * lone) // 2
    early = width * EARLY // 32
    return quarter, lone, both, early, 2 * quarter - early


def parts_of(lone, both):
    return (0, lone), (lone, both // 2), (lone + both // 2, both // 2)


def chunks_of(quarter, early):
    late, first = quarter - early, (early + 128) // 256 * 128
    return (quarter, late), (early, late), (0, first), (first, early - first)


def layer_kernel(*refs):
    r = types.SimpleNamespace(**dict(zip(NAMES, refs)))
    e, t = lax.axis_index("ep"), lax.axis_index("tp")
    z, x, y, c = e // 2, e % 2, t // 2, t % 2
    tokens, width = r.token_hbm.shape
    quarter, lone, both, early, carried = sizes_of(width)
    held = lone + both
    hidden = r.gate_hbm.shape[1]
    sibling, partner, beside = (e, y * 2 + 1 - c), (e, (1 - y) * 2 + c), (z * 2 + 1 - x, t)
    at_end = (z == 0) | (z == LINE - 1)
    at_middle = (z > 0) & (z < LINE - 1)
    near = [chosen(z, [nearest_first(place)[j] for place in range(LINE)]) for j in range(LINE)]

    def copy(src, dst, send, recv, to):
        return pltpu.make_async_remote_copy(
            src_ref=src, dst_ref=dst, send_sem=send, recv_sem=recv, device_id=to, device_id_type=MESH
        )

    def aligned(start, length):
        return pl.ds(pl.multiple_of(start, 128), length)

    def lone_of(row, core):
        return aligned(row * (width - 2 * lone) + core * lone, lone)

    def both_of(core):
        return aligned(2 * lone + core * both, both)

    sections = [
        (lone_of(y, c), 0, lone),
        (both_of(c), lone, both),
        (lone_of(y, 1 - c), held, lone),
        (both_of(1 - c), held + lone, both),
        (lone_of(1 - y, c), 2 * held, lone),
        (lone_of(1 - y, 1 - c), 2 * held + lone, lone),
    ]
    mine, theirs = (y * 2 + c) * quarter, ((1 - y) * 2 + c) * quarter

    def result_columns(core):
        own, other = (y * 2 + core) * quarter, ((1 - y) * 2 + core) * quarter
        return [
            (aligned(own, quarter), 0, quarter),
            (aligned(other + early, quarter - early), quarter, quarter - early),
            (aligned(other, early), carried, early),
        ]

    pieces = [
        (r.routing_hbm, r.routing), (r.route_weight_hbm, r.route_weight), (r.token_hbm, r.token),
        (r.gain_hbm, r.gain), (r.sink_hbm, r.sink), (r.query_hbm, r.query), (r.key_hbm, r.key),
        (r.value_hbm, r.value), (r.project_hbm, r.project),
    ]
    small = len(pieces) - 1
    for columns, place, length in sections:
        for number, weights in enumerate((r.gate_hbm, r.up_hbm)):
            pieces.append(
                (
                    weights.at[columns, :],
                    r.both_weights.at[pl.ds(place, length), pl.ds(number * hidden, hidden)],
                )
            )
    for columns, place, length in result_columns(c):
        pieces.append((r.down_hbm.at[:, columns], r.down.at[pl.ds(0, hidden), pl.ds(place, length)]))
    loads = [
        pltpu.make_async_copy(src, dst, r.load_sem.at[place]) for place, (src, dst) in enumerate(pieces)
    ]
    for load in loads[:small]:
        load.start()

    barrier = pltpu.get_barrier_semaphore()
    for step in range(1, 2 * LINE):
        pl.semaphore_signal(
            barrier, inc=1, device_id=((e + step) % (2 * LINE), t), device_id_type=MESH
        )
    for other in (sibling, partner):
        pl.semaphore_signal(barrier, inc=1, device_id=other, device_id_type=MESH)

    for load in loads[:4]:
        load.wait()
    for load in loads[small:]:
        load.start()
    widened = r.token[...].astype(jnp.float32)
    scale = lax.rsqrt(jnp.mean(widened * widened, axis=-1, keepdims=True) + EPS)
    r.own[...] = (widened * scale * r.gain[...]).astype(jnp.bfloat16)

    expert = lax.broadcasted_iota(jnp.int32, (2 * LINE, tokens), 0)
    named = jnp.zeros((2 * LINE, tokens), jnp.float32)
    for k in range(TOPK):
        named = named + jnp.where(expert == r.routing[k : k + 1], r.route_weight[k : k + 1], 0.0)
    r.shares[e] = named

    ahead = (
        lax.broadcasted_iota(jnp.int32, (tokens, tokens), 0)
        <= lax.broadcasted_iota(jnp.int32, (tokens, tokens), 1)
    ).astype(jnp.float32)
    slot = (lax.broadcasted_iota(jnp.int32, (SLOTS, tokens), 0) + 1).astype(jnp.float32)

    def ranked(block):
        routed = jnp.where(r.shares[block] > 0.0, 1.0, 0.0)
        r.ranks[block] = jnp.dot(routed, ahead, preferred_element_type=jnp.float32)

    def one_hot(block, expert):
        weight = r.shares[block, pl.ds(expert, 1), :]
        here = (r.ranks[block, pl.ds(expert, 1), :] == slot) & (weight > 0.0)
        return jnp.where(here, 1.0, 0.0), jnp.sum(jnp.where(here, weight, 0.0), axis=1, keepdims=True)

    def keep_weight(at, half, found):
        r.slot_weight[at, half * SLOTS : (half + 1) * SLOTS, :] = jnp.broadcast_to(found, (SLOTS, 128))

    def prepare(at):
        ranked(at * 2 + x)
        hot, found = one_hot(at * 2 + x, e)
        keep_weight(at, 0, found)
        r.hot[at, 0:SLOTS, :] = hot.astype(jnp.bfloat16)
        r.hot[at, SLOTS : 2 * SLOTS, :] = one_hot(at * 2 + x, z * 2 + 1 - x)[0].astype(jnp.bfloat16)

    def prepare_other(at):
        ranked(at * 2 + 1 - x)
        keep_weight(at, 1, one_hot(at * 2 + 1 - x, e)[1])

    prepare(z)
    for load in loads[4:small]:
        load.wait()
    pl.semaphore_wait(barrier, 2 * LINE + 1)

    parts = parts_of(lone, both)
    start_of_both = 2 * lone + c * both
    own_columns = (
        sections[0][0], aligned(start_of_both, both // 2), aligned(start_of_both + both // 2, both // 2)
    )

    def rows_of(half):
        return pl.ds(half * SLOTS, SLOTS)

    def own_along(up, part):
        start, length = parts[part]
        return copy(
            r.own.at[:, own_columns[part]], r.dense.at[z, :, pl.ds(start, length)],
            r.own_send.at[up, part], r.along_recv.at[z, part], (e + 4 * up - 2, t),
        )

    def onward(at, part):
        start, length = parts[part]
        view = r.dense.at[at, :, pl.ds(start, length)]
        to = (jnp.where(at < z, e + 2, e - 2), t)
        return copy(view, view, r.onward_send.at[at, part], r.along_recv.at[at, part], to)

    def across(at, part):
        start, length = parts[part]
        return copy(
            r.aside.at[at, :, pl.ds(start, length)],
            r.packed.at[at, rows_of(1), pl.ds(start, length)],
            r.across_send.at[at, part], r.across_recv.at[at, part], beside,
        )

    def to_partner(at, half):
        return copy(
            r.packed.at[at, rows_of(half), pl.ds(0, lone)],
            r.packed.at[at, rows_of(half), pl.ds(2 * held, lone)],
            r.partner_send.at[at, half], r.partner_recv.at[at, half], partner,
        )

    core_parts = [(start, held + start, length) for start, length in parts]
    core_parts.append((2 * held, 2 * held + lone, lone))

    def to_sibling(at, half, kind):
        start, landing, length = core_parts[kind]
        return copy(
            r.packed.at[at, rows_of(half), pl.ds(start, length)],
            r.packed.at[at, rows_of(half), pl.ds(landing, length)],
            r.core_send.at[at, half, kind], r.core_recv.at[at, half, kind], sibling,
        )

    def share_copy(step):
        to = (e + step) % (2 * LINE)
        return copy(r.shares.at[e], r.shares.at[e], r.share_send.at[step], r.share_recv.at[e], (to, t))

    def share_in(block):
        return copy(
            r.shares.at[block], r.shares.at[block], r.share_send.at[0], r.share_recv.at[block], beside
        )

    def own_along_start(part):
        @pl.when(z < LINE - 1)
        def _():
            own_along(1, part).start()

        @pl.when(z > 0)
        def _():
            own_along(0, part).start()

    def pack_aside(part):
        start, length = parts[part]
        found = jnp.dot(
            r.hot[z, SLOTS : 2 * SLOTS, :], r.own[:, own_columns[part]],
            preferred_element_type=jnp.float32,
        )
        r.aside[z, :, start : start + length] = found.astype(jnp.bfloat16)
        across(z, part).start()

    queries = r.query_hbm.shape[0]

    def halo_copy(which):
        src = (r.key, r.value)[which].at[pl.ds(queries - WINDOW_KEYS, WINDOW_KEYS)]
        to = ((e + 1) % (2 * LINE), t)
        return copy(src, r.halo.at[which], r.halo_send.at[which], r.halo_recv.at[which], to)

    @pl.when(e < 2 * LINE - 1)
    def _():
        halo_copy(0).start()
        halo_copy(1).start()

    @pl.when(e == 0)
    def _():
        r.halo[...] = jnp.zeros_like(r.halo)

    own_along_start(0)
    for step in range(1, 2 * LINE):
        share_copy(step).start()
    pack_aside(0)
    for part in range(1, len(parts)):
        own_along_start(part)
        pack_aside(part)

    def down_copy(number):
        columns, place, length = result_columns(1 - c)[number]
        return copy(
            r.down_hbm.at[:, columns], r.down.at[pl.ds(hidden, hidden), pl.ds(place, length)],
            r.down_send.at[number], r.down_recv.at[number], sibling,
        )

    for number in range(3):
        down_copy(number).start()

    for columns, place, length in sections:
        found = jnp.dot(r.hot[z, 0:SLOTS, :], r.own[:, columns], preferred_element_type=jnp.float32)
        r.packed[z, 0:SLOTS, place : place + length] = found.astype(jnp.bfloat16)

    kv_heads = r.key_hbm.shape[1] // HEAD_SIZE
    group = r.query_hbm.shape[1] // HEAD_SIZE // kv_heads
    span = queries // 4
    here = lax.broadcasted_iota(jnp.int32, (WINDOW_KEYS, 2 * WINDOW_KEYS), 0)
    there = lax.broadcasted_iota(jnp.int32, (WINDOW_KEYS, 2 * WINDOW_KEYS), 1)

    def attend(number, kv):
        begin = number * WINDOW_KEYS
        permitted = (there > here) & (there <= here + WINDOW_KEYS)
        if number == 0:
            permitted = permitted & ((there >= WINDOW_KEYS) | (e > 0))
        lanes = slice(kv * HEAD_SIZE, (kv + 1) * HEAD_SIZE)
        if number == 0:
            keys = jnp.concatenate([r.halo[0][:, lanes], r.key[0:WINDOW_KEYS, lanes]], axis=0)
            values = jnp.concatenate([r.halo[1][:, lanes], r.value[0:WINDOW_KEYS, lanes]], axis=0)
        else:
            keys = r.key[begin - WINDOW_KEYS : begin + WINDOW_KEYS, lanes]
            values = r.value[begin - WINDOW_KEYS : begin + WINDOW_KEYS, lanes]
        for member in range(group):
            head = kv * group + member
            columns = slice(head * HEAD_SIZE, (head + 1) * HEAD_SIZE)
            scores = lax.dot_general(
                r.query[begin : begin + WINDOW_KEYS, columns],
                keys,
                (((1,), (1,)), ((), ())),
                preferred_element_type=jnp.float32,
            ) * HEAD_SIZE ** (-0.5)
            scores = jnp.where(permitted, scores, -jnp.inf)
            sink = r.sink[head]
            highest = jnp.maximum(jnp.max(scores, axis=-1, keepdims=True), sink)
            numerator = jnp.exp(scores - highest)
            denominator = jnp.sum(numerator, axis=-1, keepdims=True) + jnp.exp(sink - highest)
            weights = (numerator / denominator).astype(jnp.bfloat16)
            found = jnp.dot(weights, values, preferred_element_type=jnp.float32)
            r.attended[begin : begin + WINDOW_KEYS, columns] = found.astype(jnp.bfloat16)

    def halo_wait():
        @pl.when(e > 0)
        def _():
            halo_copy(0).wait_recv()
            halo_copy(1).wait_recv()

    def mixed_core(half):
        at = pl.multiple_of((half * 2 + 1 - c) * span, 16)
        return copy(
            r.mixed.at[pl.ds(at, span)], r.mixed_core.at[half],
            r.mixed_core_send.at[half], r.mixed_core_recv.at[half], sibling,
        )

    cut = span // MIXED_CUTS

    def mixed_pair(number):
        at = pl.multiple_of(((1 - y) * 2 + c) * span + number * cut, 16)
        return copy(
            r.mixed.at[pl.ds(at, cut)], r.mixed_pair.at[pl.ds(number * cut, cut)],
            r.mixed_pair_send.at[number], r.mixed_pair_recv.at[number], partner,
        )

    def mixed_rows(half):
        return pl.ds(pl.multiple_of((half * 2 + c) * span, 16), span)

    def mix():
        loads[small].wait()
        for place in range(0, width, quarter):
            columns = slice(place, place + quarter)
            r.mixed[:, columns] = jnp.dot(
                r.attended[...], r.project[:, columns], preferred_element_type=jnp.float32
            ).astype(jnp.bfloat16)
        for half in range(2):
            mixed_core(half).start()

    def mix_onward():
        for half in range(2):
            mixed_core(half).wait_recv()
            total = r.mixed[mixed_rows(half), :].astype(jnp.float32)
            r.mixed[mixed_rows(half), :] = (
                total + r.mixed_core[half].astype(jnp.float32)
            ).astype(jnp.bfloat16)

    def forward(k, part):
        onward(near[k], part).wait_recv()
        onward(near[k], part).start()

    def forward_middle(k, part):
        @pl.when(at_middle)
        def _():
            forward(k, part)

    def wait_end(k, part):
        @pl.when(at_end)
        def _():
            onward(near[k], part).wait_recv()

    def pack(k, part):
        at = near[k]
        start, length = parts[part]
        found = jnp.dot(
            r.hot[at], r.dense[at, :, start : start + length], preferred_element_type=jnp.float32
        ).astype(jnp.bfloat16)
        r.aside[at, :, start : start + length] = found[SLOTS : 2 * SLOTS]
        across(at, part).start()
        r.packed[at, 0:SLOTS, start : start + length] = found[0:SLOTS]
        if part == 0:
            to_partner(at, 0).start()
        to_sibling(at, 0, part).start()

    def take_across(k, part):
        at = near[k]
        across(at, part).wait_recv()
        if part == 0:
            to_partner(at, 1).start()
        to_sibling(at, 1, part).start()

    def take_partner(k, half):
        to_partner(near[k], half).wait_recv()
        to_sibling(near[k], half, len(parts)).start()

    def get_ready(k):
        share_in(near[k] * 2 + x).wait_recv()
        prepare(near[k])

    def get_other_ready(k):
        share_in(near[k] * 2 + 1 - x).wait_recv()
        prepare_other(near[k])

    def active_copy(at):
        return copy(
            r.active.at[at, :, pl.ds(0, hidden)], r.active.at[at, :, pl.ds(hidden, hidden)],
            r.active_send.at[at], r.active_recv.at[at], sibling,
        )

    def enter(k):
        at = near[k]
        for half in (1, 0) if k else (1,):
            for kind in range(len(core_parts)):
                to_sibling(at, half, kind).wait_recv()
        pre = jnp.dot(r.packed[at], r.both_weights[...], preferred_element_type=jnp.float32)
        gate_cut = jnp.minimum(pre[:, 0:hidden], CLAMP)
        up_pre = pre[:, hidden : 2 * hidden]
        r.active[at, :, 0:hidden] = (
            (jnp.clip(up_pre, -CLAMP, CLAMP) + 1.0) * gate_cut * jax.nn.sigmoid(SLOPE * gate_cut)
        ).astype(jnp.bfloat16)
        active_copy(at).start()

    late = quarter - early
    chunks = chunks_of(quarter, early)

    def pair_copy(at, half):
        return copy(
            r.results.at[at, rows_of(half), pl.ds(carried, early)], r.pair.at[at, rows_of(half), :],
            r.pair_send.at[at, half], r.pair_recv.at[at, half], partner,
        )

    def side_copy(at, chunk):
        start, length = chunks[chunk]
        return copy(
            r.results.at[at, rows_of(1), pl.ds(start, length)], r.side.at[at, :, pl.ds(start, length)],
            r.side_send.at[at, chunk], r.side_recv.at[at, chunk], beside,
        )

    def leave(k):
        at = near[k]
        active_copy(at).wait_recv()

        def finish(start, length):
            found = jnp.dot(
                r.active[at], r.down[:, start : start + length], preferred_element_type=jnp.float32
            )
            r.results[at, :, start : start + length] = (found * r.slot_weight[at][:, 0:1]).astype(
                jnp.bfloat16
            )

        finish(carried, early)
        if k > 1:
            send_pair(k, 1)
            send_pair(k, 0)
        for chunk in range(2):
            finish(*chunks[chunk])
            if k:
                side_copy(at, chunk).start()
        finish(0, early)

    def send_pair(k, half):
        pair_copy(near[k], half).start()

    def send_side(k):
        side_copy(near[k], 0).start()
        side_copy(near[k], 1).start()

    def take_pair(k, half):
        at = near[k]
        pair_copy(at, half).wait_recv()
        rows = slice(half * SLOTS, (half + 1) * SLOTS)
        for chunk in range(2, len(chunks)):
            columns = slice(chunks[chunk][0], chunks[chunk][0] + chunks[chunk][1])
            total = r.results[at, rows, columns].astype(jnp.float32)
            r.results[at, rows, columns] = (
                total + r.pair[at, rows, columns].astype(jnp.float32)
            ).astype(jnp.bfloat16)
            if half:
                side_copy(at, chunk).start()

    def line_copy(way, at, chunk):
        start, length = chunks[chunk]
        to = (jnp.where(at > z, e + 2, e - 2), t)
        return copy(
            r.line_out.at[at, :, pl.ds(start, length)], r.line_in.at[way, at, :, pl.ds(start, length)],
            r.line_send.at[at, chunk], r.line_recv.at[way, at, chunk], to,
        )

    last = copy(r.line_out.at[z, :, pl.ds(quarter, late)], r.last, r.last_send, r.last_recv, partner)

    def line_step(k, chunk, middle):
        at = near[k]
        start, length = chunks[chunk]
        columns = slice(start, start + length)
        side_copy(at, chunk).wait_recv()
        both_sides = jnp.concatenate([r.results[at, 0:SLOTS, columns], r.side[at, :, columns]], axis=0)
        total = lax.dot_general(
            r.hot[at], both_sides, (((0,), (0,)), ((), ())), preferred_element_type=jnp.float32
        )
        if k:
            way = jnp.where(at > z, 0, 1)
            ways = (way,) if middle else ()
        elif middle:
            ways = (0, 1)
        else:
            ways = (jnp.where(z == 0, 1, 0),)
        for way in ways:
            line_copy(way, at, chunk).wait_recv()
            total = total + r.line_in[way, at, :, columns].astype(jnp.float32)
        if k or chunk == 0:
            r.line_out[at, :, columns] = total.astype(jnp.bfloat16)
            if k:
                line_copy(way, at, chunk).start()
            else:
                last.start()
        elif chunk == 1:
            r.final[...] = total
        else:
            r.out_kept[:, columns] = total.astype(jnp.bfloat16)
            keep_out(chunk).start()

    def arrive(k, part):
        wait_end(k, part)
        if k == 1:
            forward_middle(1, part)
        if k < LINE - 1:
            forward_middle(k + 1, part)

    def send_mixed(number):
        mixed_pair(number).start()

    def finish_mixed():
        for number in range(MIXED_CUTS):
            mixed_pair(number).wait_recv()
        total = r.mixed[mixed_rows(y), :].astype(jnp.float32)
        r.mixer_kept[...] = (total + r.mixed_pair[...].astype(jnp.float32)).astype(jnp.bfloat16)
        keep_mixer.start()

    def at_places(which, *steps):
        @pl.when(which)
        def _():
            for step in steps:
                step[0](*step[1:])

    def end_lines(k, *which):
        at_places(at_end, *[(line_step, k, chunk, False) for chunk in which])

    def middle_lines(k, *which):
        at_places(at_middle, *[(line_step, k, chunk, True) for chunk in which])

    keep_mixer = pltpu.make_async_copy(r.mixer_kept, r.mixer, r.keep_sem.at[0])

    def keep_out(chunk):
        start, length = chunks[chunk]
        view = pl.ds(start, length)
        return pltpu.make_async_copy(r.out_kept.at[:, view], r.out.at[:, view], r.keep_sem.at[chunk])

    def drain_dispatch():
        for part in range(len(parts)):
            @pl.when(z < LINE - 1)
            def _():
                own_along(1, part).wait_send()

            @pl.when(z > 0)
            def _():
                own_along(0, part).wait_send()

            @pl.when(at_middle)
            def _():
                for k in range(1, LINE):
                    onward(near[k], part).wait_send()

        @pl.when(e < 2 * LINE - 1)
        def _():
            halo_copy(0).wait_send()
            halo_copy(1).wait_send()

        for step in range(1, 2 * LINE):
            share_copy(step).wait_send()
        for number in range(3):
            down_copy(number).wait_send()
        for half in range(2):
            mixed_core(half).wait_send()
        for k in range(LINE):
            at = near[k]
            for part in range(len(parts)):
                across(at, part).wait_send()
            for half in (0, 1) if k else (1,):
                to_partner(at, half).wait_send()
                for kind in range(len(core_parts)):
                    to_sibling(at, half, kind).wait_send()
            active_copy(at).wait_send()

    def drain_return():
        for number in range(MIXED_CUTS):
            mixed_pair(number).wait_send()
        for k in range(LINE):
            for half in range(2):
                pair_copy(near[k], half).wait_send()
            for chunk in range(len(chunks)):
                side_copy(near[k], chunk).wait_send()

    attend(1, 0)
    attend(1, 1)
    take_across(0, 0)
    get_other_ready(0)
    get_ready(1)
    arrive(1, 0)
    pack(1, 0)
    halo_wait()
    attend(0, 0)
    attend(0, 1)
    take_across(0, 1)
    mix()
    arrive(1, 1)
    pack(1, 1)
    take_partner(0, 1)
    take_across(0, 2)
    mix_onward()
    arrive(1, 2)
    pack(1, 2)
    take_across(1, 0)
    send_mixed(0)
    get_other_ready(1)
    get_ready(2)
    for load in loads[small + 1 :]:
        load.wait()
    enter(0)
    take_partner(1, 0)
    take_across(1, 1)
    arrive(2, 0)
    pack(2, 0)
    for number in range(3):
        down_copy(number).wait_recv()
    leave(0)
    take_partner(1, 1)
    take_across(1, 2)
    arrive(2, 1)
    pack(2, 1)
    take_across(2, 0)
    send_mixed(1)
    enter(1)
    arrive(2, 2)
    pack(2, 2)
    take_partner(2, 0)
    take_across(2, 1)
    leave(1)
    get_ready(3)
    get_other_ready(2)
    arrive(3, 0)
    pack(3, 0)
    send_pair(1, 1)
    take_partner(2, 1)
    take_across(2, 2)
    arrive(3, 1)
    pack(3, 1)
    end_lines(1, 0, 1)
    enter(2)
    take_across(3, 0)
    send_pair(1, 0)
    arrive(3, 2)
    pack(3, 2)
    leave(2)
    take_partner(3, 0)
    take_across(3, 1)
    take_pair(1, 1)
    take_partner(3, 1)
    get_other_ready(3)
    take_across(3, 2)
    take_pair(1, 0)
    enter(3)
    end_lines(2, 0, 1)
    leave(3)
    send_mixed(2)
    send_mixed(3)
    send_pair(0, 1)
    send_pair(0, 0)
    take_pair(2, 1)
    end_lines(1, 2, 3)
    take_pair(2, 0)
    middle_lines(1, 0, 1)
    end_lines(3, 0, 1)
    end_lines(2, 2, 3)
    take_pair(3, 1)
    send_side(0)
    take_pair(3, 0)
    middle_lines(3, 0, 1)
    middle_lines(1, 2, 3)
    middle_lines(2, 0, 1)
    end_lines(3, 2, 3)
    take_pair(0, 1)
    take_pair(0, 0)
    drain_dispatch()
    middle_lines(3, 2)
    middle_lines(2, 2)
    middle_lines(3, 3)
    middle_lines(2, 3)
    finish_mixed()
    middle_lines(0, 0, 1, 2, 3)
    end_lines(0, 0, 1, 2)
    drain_return()
    end_lines(0, 3)

    last.wait_recv()
    r.out_kept[:, early:quarter] = (r.final[...] + r.last[...].astype(jnp.float32)).astype(
        jnp.bfloat16
    )
    keep_out(1).start()
    last.wait_send()
    for k in range(1, LINE):
        for chunk in range(len(chunks)):
            line_copy(0, near[k], chunk).wait_send()
    keep_mixer.wait()
    for chunk in range(1, len(chunks)):
        keep_out(chunk).wait()


def layer_call(
    rows, gain, routing, route_weight, queries, keys, values, sinks, project, gate_one, up_one, down_one
):
    tokens, width = rows.shape
    quarter, lone, both, early, carried = sizes_of(width)
    parts, chunks = len(parts_of(lone, both)), len(chunks_of(quarter, early))
    blocks = 2 * LINE
    hidden = gate_one.shape[1]
    kept = jnp.bfloat16
    dma = pltpu.SemaphoreType.DMA
    span = queries.shape[0] // 4
    stays = pl.BlockSpec(memory_space=pl.ANY)
    scratch = dict(
        token=pltpu.VMEM(rows.shape, kept),
        gain=pltpu.VMEM(gain.shape, jnp.float32),
        routing=pltpu.VMEM(routing.shape, jnp.int32),
        route_weight=pltpu.VMEM(route_weight.shape, jnp.float32),
        query=pltpu.VMEM(queries.shape, kept),
        key=pltpu.VMEM(keys.shape, kept),
        value=pltpu.VMEM(values.shape, kept),
        sink=pltpu.SMEM(sinks.shape, jnp.float32),
        own=pltpu.VMEM((tokens, width), kept),
        dense=pltpu.VMEM((LINE, tokens, lone + both), kept),
        packed=pltpu.VMEM((LINE, 2 * SLOTS, width), kept),
        aside=pltpu.VMEM((LINE, SLOTS, lone + both), kept),
        both_weights=pltpu.VMEM((width, 2 * hidden), kept),
        down=pltpu.VMEM((2 * hidden, 2 * quarter), kept),
        project=pltpu.VMEM(project.shape, kept),
        halo=pltpu.VMEM((2, WINDOW_KEYS, keys.shape[1]), kept),
        attended=pltpu.VMEM(queries.shape, kept),
        mixed=pltpu.VMEM((queries.shape[0], width), kept),
        mixed_core=pltpu.VMEM((2, span, width), kept),
        mixed_pair=pltpu.VMEM((span, width), kept),
        shares=pltpu.VMEM((blocks, 8, tokens), jnp.float32),
        ranks=pltpu.VMEM((blocks, 8, tokens), jnp.float32),
        hot=pltpu.VMEM((LINE, 2 * SLOTS, tokens), kept),
        slot_weight=pltpu.VMEM((LINE, 2 * SLOTS, 128), jnp.float32),
        active=pltpu.VMEM((LINE, 2 * SLOTS, 2 * hidden), kept),
        results=pltpu.VMEM((LINE, 2 * SLOTS, 2 * quarter), kept),
        pair=pltpu.VMEM((LINE, 2 * SLOTS, early), kept),
        side=pltpu.VMEM((LINE, SLOTS, carried), kept),
        line_out=pltpu.VMEM((LINE, tokens, carried), kept),
        line_in=pltpu.VMEM((2, LINE, tokens, carried), kept),
        last=pltpu.VMEM((tokens, quarter - early), kept),
        final=pltpu.VMEM((tokens, quarter - early), jnp.float32),
        mixer_kept=pltpu.VMEM((span, width), kept),
        out_kept=pltpu.VMEM((tokens, quarter), kept),
        keep_sem=dma((chunks,)),
        load_sem=dma((24,)),
        halo_send=dma((2,)),
        halo_recv=dma((2,)),
        mixed_core_send=dma((2,)),
        mixed_core_recv=dma((2,)),
        mixed_pair_send=dma((MIXED_CUTS,)),
        mixed_pair_recv=dma((MIXED_CUTS,)),
        share_send=dma((blocks,)),
        share_recv=dma((blocks,)),
        own_send=dma((2, parts)),
        onward_send=dma((LINE, parts)),
        along_recv=dma((LINE, parts)),
        across_send=dma((LINE, parts)),
        across_recv=dma((LINE, parts)),
        partner_send=dma((LINE, 2)),
        partner_recv=dma((LINE, 2)),
        core_send=dma((LINE, 2, parts + 1)),
        core_recv=dma((LINE, 2, parts + 1)),
        down_send=dma((3,)),
        down_recv=dma((3,)),
        active_send=dma((LINE,)),
        active_recv=dma((LINE,)),
        pair_send=dma((LINE, 2)),
        pair_recv=dma((LINE, 2)),
        side_send=dma((LINE, chunks)),
        side_recv=dma((LINE, chunks)),
        line_send=dma((LINE, chunks)),
        line_recv=dma((2, LINE, chunks)),
        last_send=dma,
        last_recv=dma,
    )
    return pl.pallas_call(
        layer_kernel,
        out_shape=(
            jax.ShapeDtypeStruct((span, width), kept),
            jax.ShapeDtypeStruct((tokens, quarter), kept),
        ),
        in_specs=[stays] * 12,
        out_specs=(stays, stays),
        scratch_shapes=[scratch[name] for name in NAMES[14:]],
        compiler_params=pltpu.CompilerParams(
            collective_id=0, has_side_effects=True, vmem_limit_bytes=60 * 1024 * 1024
        ),
        cost_estimate=pl.CostEstimate(
            flops=8 * blocks * tokens * width * hidden,
            bytes_accessed=8 * width * hidden,
            transcendentals=0,
        ),
    )(rows, gain, routing, route_weight, queries, keys, values, sinks, project, gate_one, up_one, down_one)


def shards(
    projected_queries,
    key_proj,
    projected_values,
    head_sink_logits,
    out_weight,
    expert_input,
    norm_gain,
    routing,
    route_weight,
    gate_weight,
    up_weight,
    down_weight,
):
    token_rows = expert_input.shape[0]
    experts = lax.axis_size("ep")
    capacity = max(3 * token_rows * TOPK // (2 * experts), 2)
    col_share = D // lax.axis_size("tp")
    if (experts, lax.axis_size("tp")) == (2 * LINE, 4) and token_rows == 128:
        return layer_call(
            expert_input,
            norm_gain[None, :],
            routing.T,
            route_weight.T,
            projected_queries,
            key_proj,
            projected_values,
            head_sink_logits,
            out_weight,
            gate_weight[0],
            up_weight[0],
            down_weight[0],
        )
    widened = expert_input.astype(jnp.float32)
    normed = (
        widened
        * lax.rsqrt(jnp.mean(widened * widened, axis=-1, keepdims=True) + EPS)
        * norm_gain[None, :]
    ).astype(jnp.bfloat16)
    query_rows = projected_queries.shape[0]
    kv_heads = key_proj.shape[1] // HEAD_SIZE
    heads_per_group = projected_queries.shape[1] // HEAD_SIZE // kv_heads
    count_of_blocks = query_rows // WINDOW_KEYS
    prior_key, prior_value = passed_along(
        (key_proj[query_rows - WINDOW_KEYS :], projected_values[query_rows - WINDOW_KEYS :]),
        "ep",
        1,
    )
    key_all = jnp.concatenate([prior_key, key_proj], axis=0)
    value_all = jnp.concatenate([prior_value, projected_values], axis=0)
    window_keys = jnp.concatenate(
        [
            key_all[:-WINDOW_KEYS].reshape(count_of_blocks, WINDOW_KEYS, kv_heads, HEAD_SIZE),
            key_all[WINDOW_KEYS:].reshape(count_of_blocks, WINDOW_KEYS, kv_heads, HEAD_SIZE),
        ],
        axis=1,
    )
    window_values = jnp.concatenate(
        [
            value_all[:-WINDOW_KEYS].reshape(count_of_blocks, WINDOW_KEYS, kv_heads, HEAD_SIZE),
            value_all[WINDOW_KEYS:].reshape(count_of_blocks, WINDOW_KEYS, kv_heads, HEAD_SIZE),
        ],
        axis=1,
    )
    query_blocks = projected_queries.reshape(
        count_of_blocks, WINDOW_KEYS, kv_heads, heads_per_group, HEAD_SIZE
    )
    scores = jnp.einsum(
        "nqhgd,nshd->nhgqs", query_blocks, window_keys, preferred_element_type=jnp.float32
    ) * HEAD_SIZE ** (-0.5)
    offset = lax.axis_index("ep") * query_rows
    block_ids = jnp.arange(count_of_blocks)[:, None, None] * WINDOW_KEYS + offset
    query_pos = block_ids + jnp.arange(WINDOW_KEYS)[None, :, None]
    key_pos = block_ids - WINDOW_KEYS + jnp.arange(2 * WINDOW_KEYS)[None, None, :]
    permitted_mask = (key_pos <= query_pos) & (query_pos - key_pos < WINDOW_KEYS) & (key_pos >= 0)
    scores = jnp.where(permitted_mask[:, None, None, :, :], scores, -jnp.inf)
    sink_col = head_sink_logits.reshape(kv_heads, heads_per_group)[None, :, :, None, None]
    highest = jnp.maximum(jnp.max(scores, axis=-1, keepdims=True), sink_col)
    numerator = jnp.exp(scores - highest)
    denominator = jnp.sum(numerator, axis=-1, keepdims=True) + jnp.exp(sink_col - highest)
    weights = (numerator / denominator).astype(jnp.bfloat16)
    attended = jnp.einsum(
        "nhgqs,nshd->nqhgd", weights, window_values, preferred_element_type=jnp.float32
    )
    attended = attended.astype(jnp.bfloat16).reshape(
        query_rows, kv_heads * heads_per_group * HEAD_SIZE
    )
    mixer_output = lax.psum_scatter(
        jnp.dot(attended, out_weight, preferred_element_type=jnp.float32).astype(jnp.bfloat16),
        "tp",
        scatter_dimension=0,
        tiled=True,
    )
    flat_ids = routing.reshape(-1)
    onehot = (flat_ids[:, None] == jnp.arange(experts, dtype=jnp.int32)[None, :]).astype(jnp.int32)
    rank_in = jnp.cumsum(onehot, axis=0) - 1
    target = flat_ids * capacity + jnp.sum(rank_in * onehot, axis=1)
    tok_ids = jnp.arange(token_rows * TOPK) // TOPK
    slot_tok = jnp.full((experts * capacity,), token_rows, jnp.int32).at[target].set(tok_ids)
    gate_one = gate_weight[0]
    up_one = up_weight[0]
    own_cols = lax.dynamic_slice_in_dim(normed, lax.axis_index("tp") * col_share, col_share, 1)
    extended = jnp.concatenate([own_cols, jnp.zeros((1, col_share), jnp.bfloat16)], axis=0)
    outgoing = jnp.take(extended, slot_tok, axis=0).reshape(experts, capacity, col_share)
    arrived = lax.all_to_all(outgoing, "ep", split_axis=0, concat_axis=0, tiled=True).reshape(
        experts * capacity, col_share
    )
    portion = lax.all_gather(arrived, "tp", axis=1, tiled=True)
    gate_pre = jnp.dot(portion, gate_one, preferred_element_type=jnp.float32)
    up_pre = jnp.dot(portion, up_one, preferred_element_type=jnp.float32)
    gate_cut = jnp.minimum(gate_pre, CLAMP)
    activated = (
        (jnp.clip(up_pre, -CLAMP, CLAMP) + 1.0) * gate_cut * jax.nn.sigmoid(SLOPE * gate_cut)
    ).astype(jnp.bfloat16)
    partial_value = jnp.dot(activated, down_weight[0], preferred_element_type=jnp.float32)
    expert_result = lax.psum_scatter(
        partial_value.astype(jnp.bfloat16), "tp", scatter_dimension=1, tiled=True
    )
    returned = lax.all_to_all(
        expert_result.reshape(experts, capacity, col_share),
        "ep",
        split_axis=0,
        concat_axis=0,
        tiled=True,
    )
    picked = jnp.take(returned.reshape(experts * capacity, col_share), target, axis=0)
    picked = picked.astype(jnp.float32).reshape(token_rows, TOPK, col_share)
    expert_output = jnp.sum(picked * route_weight[:, :, None], axis=1).astype(jnp.bfloat16)
    return (mixer_output, expert_output)


def solution(mesh):
    placed = (
        P("ep", "tp"),
        P("ep", "tp"),
        P("ep", "tp"),
        P("tp"),
        P("tp", None),
        P("ep", None),
        P(),
        P("ep", None),
        P("ep", None),
        P("ep", None, "tp"),
        P("ep", None, "tp"),
        P("ep", "tp", None),
    )
    return jax.shard_map(
        shards,
        mesh=mesh,
        in_specs=placed,
        out_specs=(P(("ep", "tp"), None), P("ep", "tp")),
        check_vma=False,
    )
```

time: 114 us -> 83.4 us (0.73)
  Pallas kernels: 108 us -> 79 us
    pallas_call x1, Pallas kernels: 108 us -> 79 us  [layer_call(): pl.pallas_call(layer_kernel, out_shape=(jax.ShapeDtypeStruct((span, width...]
where the time goes in v1:
time: 83.4 us; the launch traced here: 83.2 us
  Pallas kernels  79 us (95%)
  local copies, waits for them, and re-layouts  3.54 us (4%)
    pallas_call x1, Pallas kernels, layer_call(): pl.pallas_call(layer_kernel, out_shape=(jax.ShapeDtypeStruct((span, width...  79 us
    unnamed x2, local copies, waits for them, and re-layouts  3.54 us

profile of v1, /device:TPU:0, one launch (start us, length us, event | category | flops | bytes accessed | tf_op | source)
XLA Modules:
  0.0 83.2 jit_solution(10653472366727527159)
XLA Ops:
  0.6 79.0 %shard_map.131 = (bf16[64,4096]{1,0:T(8,128)(2,1)}, bf16[128,1024]{1,0:T(8,128)(2,1)}) custom-call(bf16[128,4096]{1,0:T(8,128)(2,1)} %refs_0_.1, f32[1,4096]{1,0:T(1,128)} %bitcast.9, s32[4,128]{1,0:T(4,128)} %bitcast.10, f32[4,128]{1,0:T(4,128)} %bitcast.11, bf16[256,512]{1,0:T(8,128)(2,1)} %refs_4_.1, bf16[256,128]{1,0:T(8,128)(2,1)} %refs_5_.1, ...), custom_call_target="tpu_custom_call" | custom-call | flops 8589934592 | bytes 8388608 | tf_op jit(solution)/shard_map/pallas_call | solution.py:831
  79.7 1.9 %copy.16 = bf16[64,4096]{1,0:T(8,128)(2,1)} copy(bf16[64,4096]{1,0:T(8,128)(2,1)} %get-tuple-element.4) | data formatting | bytes 1048576
  81.6 1.7 %copy.17 = bf16[128,1024]{1,0:T(8,128)(2,1)} copy(bf16[128,1024]{1,0:T(8,128)(2,1)} %get-tuple-element.5) | data formatting | bytes 524288

commit v2 on v1

--- a/solution.py
+++ b/solution.py
@@ -37,7 +37,7 @@
     "token", "gain", "routing", "route_weight", "query", "key", "value", "sink", "own", "dense",
     "packed", "aside", "both_weights", "down", "project", "halo", "attended", "mixed",
     "mixed_core", "mixed_pair", "shares", "ranks", "hot", "slot_weight", "active", "results",
-    "pair", "side", "line_out", "line_in", "last", "final", "mixer_kept", "out_kept", "keep_sem", "load_sem", "halo_send", "halo_recv",
+    "pair", "side", "line_out", "line_in", "last", "final", "load_sem", "halo_send", "halo_recv",
     "mixed_core_send", "mixed_core_recv", "mixed_pair_send", "mixed_pair_recv", "share_send",
     "share_recv", "own_send", "onward_send", "along_recv", "across_send", "across_recv",
     "partner_send", "partner_recv", "core_send", "core_recv", "down_send", "down_recv",
@@ -133,13 +133,20 @@
                     r.both_weights.at[pl.ds(place, length), pl.ds(number * hidden, hidden)],
                 )
             )
-    for columns, place, length in result_columns(c):
-        pieces.append((r.down_hbm.at[:, columns], r.down.at[pl.ds(0, hidden), pl.ds(place, length)]))
     loads = [
-        pltpu.make_async_copy(src, dst, r.load_sem.at[place]) for place, (src, dst) in enumerate(pieces)
+        pltpu.make_async_copy(src, dst, r.load_sem.at[min(place, small + 1)])
+        for place, (src, dst) in enumerate(pieces)
     ]
     for load in loads[:small]:
         load.start()
+
+    down_loads = [
+        pltpu.make_async_copy(
+            r.down_hbm.at[:, columns], r.down.at[pl.ds(0, hidden), pl.ds(place, length)],
+            r.load_sem.at[small + 2],
+        )
+        for columns, place, length in result_columns(c)
+    ]
 
     barrier = pltpu.get_barrier_semaphore()
     for step in range(1, 2 * LINE):
@@ -151,7 +158,7 @@
 
     for load in loads[:4]:
         load.wait()
-    for load in loads[small:]:
+    for load in loads[small:] + down_loads:
         load.start()
     widened = r.token[...].astype(jnp.float32)
     scale = lax.rsqrt(jnp.mean(widened * widened, axis=-1, keepdims=True) + EPS)
@@ -210,28 +217,28 @@
         start, length = parts[part]
         return copy(
             r.own.at[:, own_columns[part]], r.dense.at[z, :, pl.ds(start, length)],
-            r.own_send.at[up, part], r.along_recv.at[z, part], (e + 4 * up - 2, t),
+            r.own_send.at[up], r.along_recv.at[z, part], (e + 4 * up - 2, t),
         )
 
     def onward(at, part):
         start, length = parts[part]
         view = r.dense.at[at, :, pl.ds(start, length)]
         to = (jnp.where(at < z, e + 2, e - 2), t)
-        return copy(view, view, r.onward_send.at[at, part], r.along_recv.at[at, part], to)
+        return copy(view, view, r.onward_send.at[at], r.along_recv.at[at, part], to)
 
     def across(at, part):
         start, length = parts[part]
         return copy(
             r.aside.at[at, :, pl.ds(start, length)],
             r.packed.at[at, rows_of(1), pl.ds(start, length)],
-            r.across_send.at[at, part], r.across_recv.at[at, part], beside,
+            r.across_send.at[at], r.across_recv.at[at, part], beside,
         )
 
     def to_partner(at, half):
         return copy(
             r.packed.at[at, rows_of(half), pl.ds(0, lone)],
             r.packed.at[at, rows_of(half), pl.ds(2 * held, lone)],
-            r.partner_send.at[at, half], r.partner_recv.at[at, half], partner,
+            r.partner_send.at[at], r.partner_recv.at[at, half], partner,
         )
 
     core_parts = [(start, held + start, length) for start, length in parts]
@@ -242,16 +249,16 @@
         return copy(
             r.packed.at[at, rows_of(half), pl.ds(start, length)],
             r.packed.at[at, rows_of(half), pl.ds(landing, length)],
-            r.core_send.at[at, half, kind], r.core_recv.at[at, half, kind], sibling,
+            r.core_send.at[at], r.core_recv.at[at], sibling,
         )
 
     def share_copy(step):
         to = (e + step) % (2 * LINE)
-        return copy(r.shares.at[e], r.shares.at[e], r.share_send.at[step], r.share_recv.at[e], (to, t))
+        return copy(r.shares.at[e], r.shares.at[e], r.share_send, r.share_recv.at[e], (to, t))
 
     def share_in(block):
         return copy(
-            r.shares.at[block], r.shares.at[block], r.share_send.at[0], r.share_recv.at[block], beside
+            r.shares.at[block], r.shares.at[block], r.share_send, r.share_recv.at[block], beside
         )
 
     def own_along_start(part):
@@ -277,7 +284,7 @@
     def halo_copy(which):
         src = (r.key, r.value)[which].at[pl.ds(queries - WINDOW_KEYS, WINDOW_KEYS)]
         to = ((e + 1) % (2 * LINE), t)
-        return copy(src, r.halo.at[which], r.halo_send.at[which], r.halo_recv.at[which], to)
+        return copy(src, r.halo.at[which], r.halo_send, r.halo_recv.at[which], to)
 
     @pl.when(e < 2 * LINE - 1)
     def _():
@@ -300,7 +307,7 @@
         columns, place, length = result_columns(1 - c)[number]
         return copy(
             r.down_hbm.at[:, columns], r.down.at[pl.ds(hidden, hidden), pl.ds(place, length)],
-            r.down_send.at[number], r.down_recv.at[number], sibling,
+            r.down_send, r.down_recv, sibling,
         )
 
     for number in range(3):
@@ -356,7 +363,7 @@
         at = pl.multiple_of((half * 2 + 1 - c) * span, 16)
         return copy(
             r.mixed.at[pl.ds(at, span)], r.mixed_core.at[half],
-            r.mixed_core_send.at[half], r.mixed_core_recv.at[half], sibling,
+            r.mixed_core_send, r.mixed_core_recv.at[half], sibling,
         )
 
     cut = span // MIXED_CUTS
@@ -365,7 +372,7 @@
         at = pl.multiple_of(((1 - y) * 2 + c) * span + number * cut, 16)
         return copy(
             r.mixed.at[pl.ds(at, cut)], r.mixed_pair.at[pl.ds(number * cut, cut)],
-            r.mixed_pair_send.at[number], r.mixed_pair_recv.at[number], partner,
+            r.mixed_pair_send, r.mixed_pair_recv.at[number], partner,
         )
 
     def mixed_rows(half):
@@ -443,9 +450,9 @@
 
     def enter(k):
         at = near[k]
-        for half in (1, 0) if k else (1,):
-            for kind in range(len(core_parts)):
-                to_sibling(at, half, kind).wait_recv()
+        rows = pl.ds(0, 2 * SLOTS) if k else pl.ds(0, SLOTS)
+        arrived = r.packed.at[at, rows, pl.ds(0, held + lone)]
+        copy(arrived, arrived, r.core_send.at[at], r.core_recv.at[at], sibling).wait_recv()
         pre = jnp.dot(r.packed[at], r.both_weights[...], preferred_element_type=jnp.float32)
         gate_cut = jnp.minimum(pre[:, 0:hidden], CLAMP)
         up_pre = pre[:, hidden : 2 * hidden]
@@ -460,14 +467,14 @@
     def pair_copy(at, half):
         return copy(
             r.results.at[at, rows_of(half), pl.ds(carried, early)], r.pair.at[at, rows_of(half), :],
-            r.pair_send.at[at, half], r.pair_recv.at[at, half], partner,
+            r.pair_send.at[at], r.pair_recv.at[at, half], partner,
         )
 
     def side_copy(at, chunk):
         start, length = chunks[chunk]
         return copy(
             r.results.at[at, rows_of(1), pl.ds(start, length)], r.side.at[at, :, pl.ds(start, length)],
-            r.side_send.at[at, chunk], r.side_recv.at[at, chunk], beside,
+            r.side_send.at[at], r.side_recv.at[at, chunk], beside,
         )
 
     def leave(k):
@@ -517,7 +524,7 @@
         to = (jnp.where(at > z, e + 2, e - 2), t)
         return copy(
             r.line_out.at[at, :, pl.ds(start, length)], r.line_in.at[way, at, :, pl.ds(start, length)],
-            r.line_send.at[at, chunk], r.line_recv.at[way, at, chunk], to,
+            r.line_send.at[at], r.line_recv.at[way, at, chunk], to,
         )
 
     last = copy(r.line_out.at[z, :, pl.ds(quarter, late)], r.last, r.last_send, r.last_recv, partner)
@@ -550,8 +557,7 @@
         elif chunk == 1:
             r.final[...] = total
         else:
-            r.out_kept[:, columns] = total.astype(jnp.bfloat16)
-            keep_out(chunk).start()
+            r.out[:, columns] = total.astype(jnp.bfloat16)
 
     def arrive(k, part):
         wait_end(k, part)
@@ -560,6 +566,12 @@
         if k < LINE - 1:
             forward_middle(k + 1, part)
 
+    def end_packs(k, part):
+        at_places(at_end, (pack, k, part))
+
+    def middle_packs(k, part):
+        at_places(at_middle, (pack, k, part))
+
     def send_mixed(number):
         mixed_pair(number).start()
 
@@ -567,8 +579,7 @@
         for number in range(MIXED_CUTS):
             mixed_pair(number).wait_recv()
         total = r.mixed[mixed_rows(y), :].astype(jnp.float32)
-        r.mixer_kept[...] = (total + r.mixed_pair[...].astype(jnp.float32)).astype(jnp.bfloat16)
-        keep_mixer.start()
+        r.mixer[...] = (total + r.mixed_pair[...].astype(jnp.float32)).astype(jnp.bfloat16)
 
     def at_places(which, *steps):
         @pl.when(which)
@@ -582,57 +593,43 @@
     def middle_lines(k, *which):
         at_places(at_middle, *[(line_step, k, chunk, True) for chunk in which])
 
-    keep_mixer = pltpu.make_async_copy(r.mixer_kept, r.mixer, r.keep_sem.at[0])
-
-    def keep_out(chunk):
-        start, length = chunks[chunk]
-        view = pl.ds(start, length)
-        return pltpu.make_async_copy(r.out_kept.at[:, view], r.out.at[:, view], r.keep_sem.at[chunk])
+    def sent(view, semaphore):
+        copy(view, view, semaphore, semaphore, sibling).wait_send()
 
     def drain_dispatch():
-        for part in range(len(parts)):
-            @pl.when(z < LINE - 1)
-            def _():
-                own_along(1, part).wait_send()
-
-            @pl.when(z > 0)
-            def _():
-                own_along(0, part).wait_send()
-
-            @pl.when(at_middle)
-            def _():
-                for k in range(1, LINE):
-                    onward(near[k], part).wait_send()
+        @pl.when(z < LINE - 1)
+        def _():
+            sent(r.dense.at[0], r.own_send.at[1])
+
+        @pl.when(z > 0)
+        def _():
+            sent(r.dense.at[0], r.own_send.at[0])
+
+        @pl.when(at_middle)
+        def _():
+            for k in range(1, LINE):
+                sent(r.dense.at[near[k]], r.onward_send.at[near[k]])
 
         @pl.when(e < 2 * LINE - 1)
         def _():
-            halo_copy(0).wait_send()
-            halo_copy(1).wait_send()
-
-        for step in range(1, 2 * LINE):
-            share_copy(step).wait_send()
-        for number in range(3):
-            down_copy(number).wait_send()
-        for half in range(2):
-            mixed_core(half).wait_send()
+            sent(r.halo, r.halo_send)
+
+        sent(r.shares.at[pl.ds(0, 2 * LINE - 1)], r.share_send)
+        sent(r.down.at[pl.ds(0, hidden)], r.down_send)
+        sent(r.mixed_core, r.mixed_core_send)
         for k in range(LINE):
             at = near[k]
-            for part in range(len(parts)):
-                across(at, part).wait_send()
-            for half in (0, 1) if k else (1,):
-                to_partner(at, half).wait_send()
-                for kind in range(len(core_parts)):
-                    to_sibling(at, half, kind).wait_send()
+            sent(r.aside.at[at], r.across_send.at[at])
+            rows = pl.ds(0, 2 * SLOTS) if k else pl.ds(0, SLOTS)
+            sent(r.packed.at[at, rows, pl.ds(0, lone)], r.partner_send.at[at])
+            sent(r.packed.at[at, rows, pl.ds(0, held + lone)], r.core_send.at[at])
             active_copy(at).wait_send()
 
     def drain_return():
-        for number in range(MIXED_CUTS):
-            mixed_pair(number).wait_send()
-        for k in range(LINE):
-            for half in range(2):
-                pair_copy(near[k], half).wait_send()
-            for chunk in range(len(chunks)):
-                side_copy(near[k], chunk).wait_send()
+        sent(r.mixed_pair, r.mixed_pair_send)
+        for at in range(LINE):
+            sent(r.pair.at[at], r.pair_send.at[at])
+            sent(r.side.at[at], r.side_send.at[at])
 
     attend(1, 0)
     attend(1, 1)
@@ -653,100 +650,103 @@
     mix_onward()
     arrive(1, 2)
     pack(1, 2)
+    get_ready(2)
+    middle_packs(2, 0)
+    middle_packs(2, 1)
+    middle_packs(2, 2)
     take_across(1, 0)
     send_mixed(0)
     get_other_ready(1)
-    get_ready(2)
-    for load in loads[small + 1 :]:
-        load.wait()
+    pltpu.make_async_copy(r.both_weights, r.both_weights, r.load_sem.at[small + 1]).wait()
+    arrived = r.down.at[pl.ds(0, hidden)]
+    pltpu.make_async_copy(arrived, arrived, r.load_sem.at[small + 2]).wait()
+    copy(arrived, arrived, r.down_send, r.down_recv, sibling).wait_recv()
     enter(0)
     take_partner(1, 0)
     take_across(1, 1)
     arrive(2, 0)
-    pack(2, 0)
-    for number in range(3):
-        down_copy(number).wait_recv()
+    end_packs(2, 0)
+    get_ready(3)
+    middle_packs(3, 0)
     leave(0)
+    take_across(1, 2)
     take_partner(1, 1)
-    take_across(1, 2)
     arrive(2, 1)
-    pack(2, 1)
+    end_packs(2, 1)
+    middle_packs(3, 1)
     take_across(2, 0)
     send_mixed(1)
     enter(1)
     arrive(2, 2)
-    pack(2, 2)
+    end_packs(2, 2)
+    middle_packs(3, 2)
+    take_across(2, 1)
     take_partner(2, 0)
-    take_across(2, 1)
     leave(1)
-    get_ready(3)
     get_other_ready(2)
     arrive(3, 0)
-    pack(3, 0)
+    end_packs(3, 0)
     send_pair(1, 1)
+    take_across(2, 2)
     take_partner(2, 1)
-    take_across(2, 2)
     arrive(3, 1)
-    pack(3, 1)
-    end_lines(1, 0, 1)
+    end_packs(3, 1)
     enter(2)
     take_across(3, 0)
     send_pair(1, 0)
     arrive(3, 2)
-    pack(3, 2)
+    end_packs(3, 2)
+    end_lines(1, 0, 1)
     leave(2)
-    take_partner(3, 0)
     take_across(3, 1)
     take_pair(1, 1)
+    take_partner(3, 0)
+    take_across(3, 2)
+    take_pair(1, 0)
     take_partner(3, 1)
     get_other_ready(3)
-    take_across(3, 2)
-    take_pair(1, 0)
+    end_lines(2, 0, 1)
     enter(3)
-    end_lines(2, 0, 1)
+    end_lines(1, 2, 3)
+    take_pair(2, 1)
     leave(3)
+    send_pair(0, 1)
+    send_pair(0, 0)
     send_mixed(2)
     send_mixed(3)
-    send_pair(0, 1)
-    send_pair(0, 0)
-    take_pair(2, 1)
-    end_lines(1, 2, 3)
     take_pair(2, 0)
     middle_lines(1, 0, 1)
-    end_lines(3, 0, 1)
     end_lines(2, 2, 3)
     take_pair(3, 1)
     send_side(0)
+    end_lines(3, 0, 1)
     take_pair(3, 0)
+    middle_lines(1, 2, 3)
     middle_lines(3, 0, 1)
-    middle_lines(1, 2, 3)
-    middle_lines(2, 0, 1)
     end_lines(3, 2, 3)
+    middle_lines(2, 0)
+    middle_lines(3, 2)
+    middle_lines(2, 1)
+    middle_lines(3, 3)
     take_pair(0, 1)
     take_pair(0, 0)
     drain_dispatch()
-    middle_lines(3, 2)
-    middle_lines(2, 2)
-    middle_lines(3, 3)
-    middle_lines(2, 3)
+    middle_lines(2, 2, 3)
+    middle_lines(0, 0, 1)
+    end_lines(0, 0, 1)
     finish_mixed()
-    middle_lines(0, 0, 1, 2, 3)
-    end_lines(0, 0, 1, 2)
+    middle_lines(0, 2, 3)
+    end_lines(0, 2)
     drain_return()
     end_lines(0, 3)
 
     last.wait_recv()
-    r.out_kept[:, early:quarter] = (r.final[...] + r.last[...].astype(jnp.float32)).astype(
+    r.out[:, early:quarter] = (r.final[...] + r.last[...].astype(jnp.float32)).astype(
         jnp.bfloat16
     )
-    keep_out(1).start()
     last.wait_send()
     for k in range(1, LINE):
-        for chunk in range(len(chunks)):
-            line_copy(0, near[k], chunk).wait_send()
-    keep_mixer.wait()
-    for chunk in range(1, len(chunks)):
-        keep_out(chunk).wait()
+        sent(r.line_out.at[near[k]], r.line_send.at[near[k]])
 
 
 def layer_call(
@@ -761,6 +761,7 @@
     dma = pltpu.SemaphoreType.DMA
     span = queries.shape[0] // 4
     stays = pl.BlockSpec(memory_space=pl.ANY)
+    in_vmem = pl.BlockSpec(memory_space=pltpu.VMEM)
     scratch = dict(
         token=pltpu.VMEM(rows.shape, kept),
         gain=pltpu.VMEM(gain.shape, jnp.float32),
@@ -794,36 +795,33 @@
         line_in=pltpu.VMEM((2, LINE, tokens, carried), kept),
         last=pltpu.VMEM((tokens, quarter - early), kept),
         final=pltpu.VMEM((tokens, quarter - early), jnp.float32),
-        mixer_kept=pltpu.VMEM((span, width), kept),
-        out_kept=pltpu.VMEM((tokens, quarter), kept),
-        keep_sem=dma((chunks,)),
-        load_sem=dma((24,)),
-        halo_send=dma((2,)),
+        load_sem=dma((11,)),
+        halo_send=dma,
         halo_recv=dma((2,)),
-        mixed_core_send=dma((2,)),
+        mixed_core_send=dma,
         mixed_core_recv=dma((2,)),
-        mixed_pair_send=dma((MIXED_CUTS,)),
+        mixed_pair_send=dma,
         mixed_pair_recv=dma((MIXED_CUTS,)),
-        share_send=dma((blocks,)),
+        share_send=dma,
         share_recv=dma((blocks,)),
-        own_send=dma((2, parts)),
-        onward_send=dma((LINE, parts)),
+        own_send=dma((2,)),
+        onward_send=dma((LINE,)),
         along_recv=dma((LINE, parts)),
-        across_send=dma((LINE, parts)),
+        across_send=dma((LINE,)),
         across_recv=dma((LINE, parts)),
-        partner_send=dma((LINE, 2)),
+        partner_send=dma((LINE,)),
         partner_recv=dma((LINE, 2)),
-        core_send=dma((LINE, 2, parts + 1)),
-        core_recv=dma((LINE, 2, parts + 1)),
-        down_send=dma((3,)),
-        down_recv=dma((3,)),
+        core_send=dma((LINE,)),
+        core_recv=dma((LINE,)),
+        down_send=dma,
+        down_recv=dma,
         active_send=dma((LINE,)),
         active_recv=dma((LINE,)),
-        pair_send=dma((LINE, 2)),
+        pair_send=dma((LINE,)),
         pair_recv=dma((LINE, 2)),
-        side_send=dma((LINE, chunks)),
+        side_send=dma((LINE,)),
         side_recv=dma((LINE, chunks)),
-        line_send=dma((LINE, chunks)),
+        line_send=dma((LINE,)),
         line_recv=dma((2, LINE, chunks)),
         last_send=dma,
         last_recv=dma,
@@ -831,11 +829,11 @@
     return pl.pallas_call(
         layer_kernel,
         out_shape=(
-            jax.ShapeDtypeStruct((span, width), kept),
-            jax.ShapeDtypeStruct((tokens, quarter), kept),
+            pltpu.VMEM((span, width), kept),
+            pltpu.VMEM((tokens, quarter), kept),
         ),
         in_specs=[stays] * 12,
-        out_specs=(stays, stays),
+        out_specs=(in_vmem, in_vmem),
         scratch_shapes=[scratch[name] for name in NAMES[14:]],
         compiler_params=pltpu.CompilerParams(
             collective_id=0, has_side_effects=True, vmem_limit_bytes=60 * 1024 * 1024

time: 83.4 us -> 76.7 us (0.920)
  Pallas kernels: 79 us -> 74.4 us
  local copies, waits for them, and re-layouts: 3.54 us -> 1.5 us
    pallas_call x1, Pallas kernels: 79 us -> 74.4 us  [layer_call(): pl.pallas_call(layer_kernel, out_shape=(pltpu.VMEM((span, width), kept),...]
    unnamed x2, local copies, waits for them, and re-layouts: 3.54 us -> 1.5 us
where the time goes in v2:
time: 76.7 us; the launch traced here: 76.5 us
  Pallas kernels  74.4 us (97%)
  local copies, waits for them, and re-layouts  1.5 us (2%)
    pallas_call x1, Pallas kernels, layer_call(): pl.pallas_call(layer_kernel, out_shape=(pltpu.VMEM((span, width), kept),...  74.4 us

profile of v2, /device:TPU:0, one launch (start us, length us, event | category | flops | bytes accessed | tf_op | source)
XLA Modules:
  0.0 76.5 jit_solution(5860801244835074029)
XLA Ops:
  0.6 74.4 %shard_map.131 = (bf16[64,4096]{1,0:T(8,128)(2,1)S(1)}, bf16[128,1024]{1,0:T(8,128)(2,1)S(1)}) custom-call(bf16[128,4096]{1,0:T(8,128)(2,1)} %refs_0_.1, f32[1,4096]{1,0:T(1,128)} %bitcast.9, s32[4,128]{1,0:T(4,128)} %bitcast.10, f32[4,128]{1,0:T(4,128)} %bitcast.11, bf16[256,512]{1,0:T(8,128)(2,1)} %refs_4_.1, bf16[256,128]{1,0:T(8,128)(2,1)} %refs_5_.1, ...), custom_call_target="tpu_custom_call" | custom-call | flops 8589934592 | bytes 8388608 | tf_op jit(solution)/shard_map/pallas_call | solution.py:829
  75.0 0.8 %copy.16 = bf16[64,4096]{1,0:T(8,128)(2,1)} copy(bf16[64,4096]{1,0:T(8,128)(2,1)S(1)} %get-tuple-element.2) | data formatting | bytes 1048576
  75.8 0.7 copy.17

commit v3 on v2

--- a/solution.py
+++ b/solution.py
@@ -199,7 +199,6 @@
         ranked(at * 2 + 1 - x)
         keep_weight(at, 1, one_hot(at * 2 + 1 - x, e)[1])
 
-    prepare(z)
     for load in loads[4:small]:
         load.wait()
     pl.semaphore_wait(barrier, 2 * LINE + 1)
@@ -298,9 +297,10 @@
     own_along_start(0)
     for step in range(1, 2 * LINE):
         share_copy(step).start()
-    pack_aside(0)
     for part in range(1, len(parts)):
         own_along_start(part)
+    prepare(z)
+    for part in range(len(parts)):
         pack_aside(part)
 
     def down_copy(number):
@@ -400,15 +400,8 @@
         onward(near[k], part).wait_recv()
         onward(near[k], part).start()
 
-    def forward_middle(k, part):
-        @pl.when(at_middle)
-        def _():
-            forward(k, part)
-
-    def wait_end(k, part):
-        @pl.when(at_end)
-        def _():
-            onward(near[k], part).wait_recv()
+    def take_end(k, part):
+        onward(near[k], part).wait_recv()
 
     def pack(k, part):
         at = near[k]
@@ -490,9 +483,6 @@
             )
 
         finish(carried, early)
-        if k > 1:
-            send_pair(k, 1)
-            send_pair(k, 0)
         for chunk in range(2):
             finish(*chunks[chunk])
             if k:
@@ -559,18 +549,13 @@
         else:
             r.out[:, columns] = total.astype(jnp.bfloat16)
 
-    def arrive(k, part):
-        wait_end(k, part)
-        if k == 1:
-            forward_middle(1, part)
-        if k < LINE - 1:
-            forward_middle(k + 1, part)
-
-    def end_packs(k, part):
-        at_places(at_end, (pack, k, part))
-
-    def middle_packs(k, part):
-        at_places(at_middle, (pack, k, part))
+    def wait_expert_weights():
+        pltpu.make_async_copy(r.both_weights, r.both_weights, r.load_sem.at[small + 1]).wait()
+
+    def wait_down_weights():
+        arrived = r.down.at[pl.ds(0, hidden)]
+        pltpu.make_async_copy(arrived, arrived, r.load_sem.at[small + 2]).wait()
+        copy(arrived, arrived, r.down_send, r.down_recv, sibling).wait_recv()
 
     def send_mixed(number):
         mixed_pair(number).start()
@@ -586,12 +571,6 @@
         def _():
             for step in steps:
                 step[0](*step[1:])
-
-    def end_lines(k, *which):
-        at_places(at_end, *[(line_step, k, chunk, False) for chunk in which])
-
-    def middle_lines(k, *which):
-        at_places(at_middle, *[(line_step, k, chunk, True) for chunk in which])
 
     def sent(view, semaphore):
         copy(view, view, semaphore, semaphore, sibling).wait_send()
@@ -631,114 +610,253 @@
             sent(r.pair.at[at], r.pair_send.at[at])
             sent(r.side.at[at], r.side_send.at[at])
 
+    at_places(
+        at_end,
+        (take_across, 0, 0),
+        (take_end, 1, 0),
+    )
+    get_ready(1)
+    at_places(
+        at_middle,
+        (forward, 2, 0),
+        (forward, 1, 0),
+    )
     attend(1, 0)
-    attend(1, 1)
-    take_across(0, 0)
-    get_other_ready(0)
-    get_ready(1)
-    arrive(1, 0)
+    at_places(at_end, (take_end, 1, 1))
     pack(1, 0)
     halo_wait()
+    attend(0, 1)
+    at_places(
+        at_end,
+        (take_across, 0, 2),
+        (pack, 1, 1),
+    )
+    attend(1, 1)
+    at_places(at_end, (take_partner, 0, 1))
+    at_places(at_middle, (take_across, 0, 0))
+    get_other_ready(0)
     attend(0, 0)
-    attend(0, 1)
-    take_across(0, 1)
+    at_places(at_end, (take_across, 1, 0))
+    at_places(at_middle, (forward, 1, 1))
+    get_ready(2)
     mix()
-    arrive(1, 1)
-    pack(1, 1)
-    take_partner(0, 1)
-    take_across(0, 2)
+    at_places(at_end, (take_end, 2, 0))
+    at_places(at_middle, (pack, 1, 1))
+    pack(2, 0)
+    at_places(
+        at_middle,
+        (take_across, 0, 2),
+        (forward, 2, 1),
+    )
+    get_other_ready(1)
+    at_places(at_end, (take_across, 0, 1))
+    at_places(at_middle, (forward, 3, 0))
+    get_ready(3)
+    at_places(
+        at_end,
+        (take_partner, 1, 0),
+        (take_end, 2, 1),
+    )
+    at_places(
+        at_middle,
+        (pack, 2, 1),
+        (pack, 3, 0),
+        (take_across, 0, 1),
+        (forward, 2, 2),
+    )
     mix_onward()
-    arrive(1, 2)
-    pack(1, 2)
-    get_ready(2)
-    middle_packs(2, 0)
-    middle_packs(2, 1)
-    middle_packs(2, 2)
-    take_across(1, 0)
-    send_mixed(0)
-    get_other_ready(1)
-    pltpu.make_async_copy(r.both_weights, r.both_weights, r.load_sem.at[small + 1]).wait()
-    arrived = r.down.at[pl.ds(0, hidden)]
-    pltpu.make_async_copy(arrived, arrived, r.load_sem.at[small + 2]).wait()
-    copy(arrived, arrived, r.down_send, r.down_recv, sibling).wait_recv()
+    at_places(
+        at_end,
+        (take_end, 1, 2),
+        (send_mixed, 1),
+        (pack, 1, 2),
+    )
+    at_places(
+        at_middle,
+        (forward, 3, 1),
+        (take_across, 1, 1),
+        (take_across, 1, 0),
+        (pack, 2, 2),
+        (take_partner, 0, 1),
+        (take_across, 2, 0),
+        (forward, 3, 2),
+        (take_partner, 3, 0),
+    )
+    get_other_ready(2)
+    at_places(at_middle, (take_across, 3, 0))
+    get_other_ready(3)
+    at_places(
+        at_end,
+        (take_end, 3, 0),
+        (pack, 3, 0),
+    )
+    at_places(
+        at_middle,
+        (take_across, 2, 1),
+        (take_partner, 1, 1),
+        (forward, 1, 2),
+        (send_mixed, 0),
+        (pack, 3, 1),
+    )
+    wait_expert_weights()
     enter(0)
-    take_partner(1, 0)
-    take_across(1, 1)
-    arrive(2, 0)
-    end_packs(2, 0)
-    get_ready(3)
-    middle_packs(3, 0)
+    at_places(
+        at_end,
+        (pack, 2, 1),
+        (take_across, 2, 0),
+        (take_across, 1, 1),
+        (take_partner, 1, 1),
+    )
+    at_places(
+        at_middle,
+        (pack, 1, 2),
+        (take_partner, 2, 0),
+        (take_partner, 1, 0),
+        (take_partner, 2, 1),
+    )
+    wait_down_weights()
     leave(0)
+    at_places(
+        at_middle,
+        (take_across, 3, 1),
+        (send_pair, 0, 1),
+        (take_partner, 3, 1),
+        (take_across, 2, 2),
+        (pack, 3, 2),
+        (send_side, 0),
+        (send_pair, 0, 0),
+    )
     take_across(1, 2)
-    take_partner(1, 1)
-    arrive(2, 1)
-    end_packs(2, 1)
-    middle_packs(3, 1)
-    take_across(2, 0)
-    send_mixed(1)
+    at_places(
+        at_end,
+        (take_end, 3, 1),
+        (take_across, 3, 0),
+        (send_mixed, 0),
+        (pack, 3, 1),
+        (take_partner, 3, 0),
+        (take_end, 3, 2),
+        (pack, 3, 2),
+    )
     enter(1)
-    arrive(2, 2)
-    end_packs(2, 2)
-    middle_packs(3, 2)
-    take_across(2, 1)
-    take_partner(2, 0)
+    at_places(at_end, (send_pair, 0, 0))
+    at_places(at_middle, (take_across, 3, 2))
     leave(1)
-    get_other_ready(2)
-    arrive(3, 0)
-    end_packs(3, 0)
+    at_places(
+        at_end,
+        (take_across, 3, 1),
+        (take_end, 2, 2),
+    )
     send_pair(1, 1)
-    take_across(2, 2)
-    take_partner(2, 1)
-    arrive(3, 1)
-    end_packs(3, 1)
+    at_places(
+        at_end,
+        (pack, 2, 2),
+        (take_partner, 3, 1),
+        (take_partner, 2, 1),
+        (take_across, 3, 2),
+    )
+    enter(3)
+    at_places(
+        at_end,
+        (take_partner, 2, 0),
+        (take_across, 2, 1),
+        (line_step, 1, 0, False),
+    )
+    at_places(at_middle, (send_pair, 1, 0))
+    leave(3)
+    at_places(
+        at_end,
+        (line_step, 1, 1, False),
+        (send_pair, 3, 1),
+    )
+    at_places(at_middle, (take_pair, 0, 0))
+    send_pair(3, 0)
+    at_places(at_end, (take_across, 2, 2))
     enter(2)
-    take_across(3, 0)
-    send_pair(1, 0)
-    arrive(3, 2)
-    end_packs(3, 2)
-    end_lines(1, 0, 1)
+    at_places(at_end, (line_step, 3, 0, False))
     leave(2)
-    take_across(3, 1)
-    take_pair(1, 1)
-    take_partner(3, 0)
-    take_across(3, 2)
-    take_pair(1, 0)
-    take_partner(3, 1)
-    get_other_ready(3)
-    end_lines(2, 0, 1)
-    enter(3)
-    end_lines(1, 2, 3)
+    at_places(
+        at_middle,
+        (send_pair, 3, 1),
+        (line_step, 3, 0, True),
+        (take_pair, 3, 0),
+        (send_pair, 2, 1),
+        (line_step, 3, 1, True),
+        (take_pair, 3, 1),
+        (send_mixed, 2),
+        (take_pair, 1, 0),
+        (take_pair, 1, 1),
+        (line_step, 2, 0, True),
+        (line_step, 1, 0, True),
+    )
+    send_pair(2, 0)
+    at_places(
+        at_end,
+        (line_step, 3, 1, False),
+        (send_pair, 2, 1),
+        (send_pair, 1, 0),
+        (take_pair, 3, 1),
+        (line_step, 2, 0, False),
+        (take_pair, 3, 0),
+        (take_pair, 0, 0),
+        (line_step, 2, 1, False),
+    )
+    at_places(at_middle, (line_step, 1, 1, True))
+    send_mixed(3)
+    at_places(
+        at_end,
+        (send_pair, 0, 1),
+        (send_mixed, 2),
+        (line_step, 3, 2, False),
+    )
+    at_places(at_middle, (send_mixed, 1))
     take_pair(2, 1)
-    leave(3)
-    send_pair(0, 1)
-    send_pair(0, 0)
-    send_mixed(2)
-    send_mixed(3)
+    at_places(
+        at_end,
+        (take_pair, 1, 1),
+        (line_step, 3, 3, False),
+    )
+    at_places(
+        at_middle,
+        (line_step, 3, 2, True),
+        (line_step, 2, 1, True),
+        (take_pair, 0, 1),
+        (line_step, 0, 0, True),
+    )
     take_pair(2, 0)
-    middle_lines(1, 0, 1)
-    end_lines(2, 2, 3)
-    take_pair(3, 1)
-    send_side(0)
-    end_lines(3, 0, 1)
-    take_pair(3, 0)
-    middle_lines(1, 2, 3)
-    middle_lines(3, 0, 1)
-    end_lines(3, 2, 3)
-    middle_lines(2, 0)
-    middle_lines(3, 2)
-    middle_lines(2, 1)
-    middle_lines(3, 3)
-    take_pair(0, 1)
-    take_pair(0, 0)
+    at_places(
+        at_end,
+        (take_pair, 1, 0),
+        (line_step, 2, 2, False),
+        (line_step, 2, 3, False),
+        (send_side, 0),
+        (line_step, 1, 2, False),
+        (line_step, 1, 3, False),
+        (take_pair, 0, 1),
+        (line_step, 0, 0, False),
+        (line_step, 0, 2, False),
+    )
+    at_places(
+        at_middle,
+        (line_step, 3, 3, True),
+        (line_step, 0, 1, True),
+        (line_step, 1, 2, True),
+        (line_step, 2, 2, True),
+    )
     drain_dispatch()
-    middle_lines(2, 2, 3)
-    middle_lines(0, 0, 1)
-    end_lines(0, 0, 1)
+    at_places(at_end, (line_step, 0, 1, False))
+    at_places(
+        at_middle,
+        (line_step, 1, 3, True),
+        (line_step, 2, 3, True),
+    )
     finish_mixed()
-    middle_lines(0, 2, 3)
-    end_lines(0, 2)
+    at_places(at_end, (line_step, 0, 3, False))
+    at_places(
+        at_middle,
+        (line_step, 0, 2, True),
+        (line_step, 0, 3, True),
+    )
     drain_return()
-    end_lines(0, 3)
 
     last.wait_recv()
     r.out[:, early:quarter] = (r.final[...] + r.last[...].astype(jnp.float32)).astype(

time: 76.7 us -> 71.6 us (0.934)
  Pallas kernels: 74.4 us -> 69.3 us
    pallas_call x1, Pallas kernels: 74.4 us -> 69.3 us  [layer_call(): pl.pallas_call(layer_kernel, out_shape=(pltpu.VMEM((span, width), kept),...]
where the time goes in v3:
time: 71.6 us; the launch traced here: 71.4 us
  Pallas kernels  69.3 us (97%)
  local copies, waits for them, and re-layouts  1.5 us (2%)
    pallas_call x1, Pallas kernels, layer_call(): pl.pallas_call(layer_kernel, out_shape=(pltpu.VMEM((span, width), kept),...  69.3 us
    unnamed x2, local copies, waits for them, and re-layouts  1.5 us

profile of v3, /device:TPU:0, one launch (start us, length us, event | category | flops | bytes accessed | tf_op | source)
XLA Modules:
  0.0 71.4 jit_solution(5727879893134443753)
XLA Ops:
  0.6 69.3 %shard_map.131 = (bf16[64,4096]{1,0:T(8,128)(2,1)S(1)}, bf16[128,1024]{1,0:T(8,128)(2,1)S(1)}) custom-call(bf16[128,4096]{1,0:T(8,128)(2,1)} %refs_0_.1, f32[1,4096]{1,0:T(1,128)} %bitcast.9, s32[4,128]{1,0:T(4,128)} %bitcast.10, f32[4,128]{1,0:T(4,128)} %bitcast.11, bf16[256,512]{1,0:T(8,128)(2,1)} %refs_4_.1, bf16[256,128]{1,0:T(8,128)(2,1)} %refs_5_.1, ...), custom_call_target="tpu_custom_call" | custom-call | flops 8589934592 | bytes 8388608 | tf_op jit(solution)/shard_map/pallas_call | solution.py:947
  69.9 0.8 %copy.16 = bf16[64,4096]{1,0:T(8,128)(2,1)} copy(bf16[64,4096]{1,0:T(8,128)(2,1)S(1)} %get-tuple-element.2) | data formatting | bytes 1048576
  70.7 0.7 copy.17

commit v4 on v3

--- a/solution.py
+++ b/solution.py
@@ -70,8 +70,9 @@
 
 
 def chunks_of(quarter, early):
-    late, first = quarter - early, (early + 128) // 256 * 128
-    return (quarter, late), (early, late), (0, first), (first, early - first)
+    late = quarter - early
+    cut = (early + 128) // 256 * 128
+    return (quarter, late), (early, late), (0, cut), (cut, early - cut)
 
 
 def layer_kernel(*refs):
@@ -120,8 +121,8 @@
         ]
 
     pieces = [
-        (r.routing_hbm, r.routing), (r.route_weight_hbm, r.route_weight), (r.token_hbm, r.token),
-        (r.gain_hbm, r.gain), (r.sink_hbm, r.sink), (r.query_hbm, r.query), (r.key_hbm, r.key),
+        (r.token_hbm, r.token), (r.gain_hbm, r.gain), (r.routing_hbm, r.routing),
+        (r.route_weight_hbm, r.route_weight), (r.sink_hbm, r.sink), (r.query_hbm, r.query), (r.key_hbm, r.key),
         (r.value_hbm, r.value), (r.project_hbm, r.project),
     ]
     small = len(pieces) - 1
@@ -156,7 +157,7 @@
     for other in (sibling, partner):
         pl.semaphore_signal(barrier, inc=1, device_id=other, device_id_type=MESH)
 
-    for load in loads[:4]:
+    for load in loads[:2]:
         load.wait()
     for load in loads[small:] + down_loads:
         load.start()
@@ -164,6 +165,8 @@
     scale = lax.rsqrt(jnp.mean(widened * widened, axis=-1, keepdims=True) + EPS)
     r.own[...] = (widened * scale * r.gain[...]).astype(jnp.bfloat16)
 
+    for load in loads[2:4]:
+        load.wait()
     expert = lax.broadcasted_iota(jnp.int32, (2 * LINE, tokens), 0)
     named = jnp.zeros((2 * LINE, tokens), jnp.float32)
     for k in range(TOPK):
@@ -223,14 +226,14 @@
         start, length = parts[part]
         view = r.dense.at[at, :, pl.ds(start, length)]
         to = (jnp.where(at < z, e + 2, e - 2), t)
-        return copy(view, view, r.onward_send.at[at], r.along_recv.at[at, part], to)
+        return copy(view, view, r.onward_send, r.along_recv.at[at, part], to)
 
     def across(at, part):
         start, length = parts[part]
         return copy(
             r.aside.at[at, :, pl.ds(start, length)],
             r.packed.at[at, rows_of(1), pl.ds(start, length)],
-            r.across_send.at[at], r.across_recv.at[at, part], beside,
+            r.across_send, r.across_recv.at[at, part], beside,
         )
 
     def to_partner(at, half):
@@ -372,7 +375,7 @@
         at = pl.multiple_of(((1 - y) * 2 + c) * span + number * cut, 16)
         return copy(
             r.mixed.at[pl.ds(at, cut)], r.mixed_pair.at[pl.ds(number * cut, cut)],
-            r.mixed_pair_send, r.mixed_pair_recv.at[number], partner,
+            r.mixed_pair_send, r.mixed_pair_recv, partner,
         )
 
     def mixed_rows(half):
@@ -438,7 +441,7 @@
     def active_copy(at):
         return copy(
             r.active.at[at, :, pl.ds(0, hidden)], r.active.at[at, :, pl.ds(hidden, hidden)],
-            r.active_send.at[at], r.active_recv.at[at], sibling,
+            r.active_send, r.active_recv.at[at], sibling,
         )
 
     def enter(k):
@@ -460,14 +463,14 @@
     def pair_copy(at, half):
         return copy(
             r.results.at[at, rows_of(half), pl.ds(carried, early)], r.pair.at[at, rows_of(half), :],
-            r.pair_send.at[at], r.pair_recv.at[at, half], partner,
+            r.pair_send, r.pair_recv.at[at, half], partner,
         )
 
     def side_copy(at, chunk):
         start, length = chunks[chunk]
         return copy(
             r.results.at[at, rows_of(1), pl.ds(start, length)], r.side.at[at, :, pl.ds(start, length)],
-            r.side_send.at[at], r.side_recv.at[at, chunk], beside,
+            r.side_send, r.side_recv.at[at, chunk], beside,
         )
 
     def leave(k):
@@ -482,12 +485,8 @@
                 jnp.bfloat16
             )
 
-        finish(carried, early)
-        for chunk in range(2):
-            finish(*chunks[chunk])
-            if k:
-                side_copy(at, chunk).start()
-        finish(0, early)
+        for start in range(0, 2 * quarter, quarter // 2):
+            finish(start, quarter // 2)
 
     def send_pair(k, half):
         pair_copy(near[k], half).start()
@@ -514,7 +513,7 @@
         to = (jnp.where(at > z, e + 2, e - 2), t)
         return copy(
             r.line_out.at[at, :, pl.ds(start, length)], r.line_in.at[way, at, :, pl.ds(start, length)],
-            r.line_send.at[at], r.line_recv.at[way, at, chunk], to,
+            r.line_send, r.line_recv.at[way, at, chunk], to,
         )
 
     last = copy(r.line_out.at[z, :, pl.ds(quarter, late)], r.last, r.last_send, r.last_recv, partner)
@@ -561,8 +560,8 @@
         mixed_pair(number).start()
 
     def finish_mixed():
-        for number in range(MIXED_CUTS):
-            mixed_pair(number).wait_recv()
+        whole = r.mixed_pair
+        copy(whole, whole, r.mixed_pair_send, r.mixed_pair_recv, partner).wait_recv()
         total = r.mixed[mixed_rows(y), :].astype(jnp.float32)
         r.mixer[...] = (total + r.mixed_pair[...].astype(jnp.float32)).astype(jnp.bfloat16)
 
@@ -586,8 +585,7 @@
 
         @pl.when(at_middle)
         def _():
-            for k in range(1, LINE):
-                sent(r.dense.at[near[k]], r.onward_send.at[near[k]])
+            sent(r.dense.at[pl.ds(0, LINE - 1)], r.onward_send)
 
         @pl.when(e < 2 * LINE - 1)
         def _():
@@ -596,19 +594,18 @@
         sent(r.shares.at[pl.ds(0, 2 * LINE - 1)], r.share_send)
         sent(r.down.at[pl.ds(0, hidden)], r.down_send)
         sent(r.mixed_core, r.mixed_core_send)
+        sent(r.aside, r.across_send)
+        sent(r.active.at[:, :, pl.ds(0, hidden)], r.active_send)
         for k in range(LINE):
             at = near[k]
-            sent(r.aside.at[at], r.across_send.at[at])
             rows = pl.ds(0, 2 * SLOTS) if k else pl.ds(0, SLOTS)
             sent(r.packed.at[at, rows, pl.ds(0, lone)], r.partner_send.at[at])
             sent(r.packed.at[at, rows, pl.ds(0, held + lone)], r.core_send.at[at])
-            active_copy(at).wait_send()
 
     def drain_return():
         sent(r.mixed_pair, r.mixed_pair_send)
-        for at in range(LINE):
-            sent(r.pair.at[at], r.pair_send.at[at])
-            sent(r.side.at[at], r.side_send.at[at])
+        sent(r.pair, r.pair_send)
+        sent(r.side, r.side_send)
 
     at_places(
         at_end,
@@ -741,6 +738,7 @@
     at_places(at_end, (send_pair, 0, 0))
     at_places(at_middle, (take_across, 3, 2))
     leave(1)
+    send_side(1)
     at_places(
         at_end,
         (take_across, 3, 1),
@@ -763,6 +761,7 @@
     )
     at_places(at_middle, (send_pair, 1, 0))
     leave(3)
+    send_side(3)
     at_places(
         at_end,
         (line_step, 1, 1, False),
@@ -774,6 +773,7 @@
     enter(2)
     at_places(at_end, (line_step, 3, 0, False))
     leave(2)
+    send_side(2)
     at_places(
         at_middle,
         (send_pair, 3, 1),
@@ -863,8 +863,7 @@
         jnp.bfloat16
     )
     last.wait_send()
-    for k in range(1, LINE):
-        sent(r.line_out.at[near[k]], r.line_send.at[near[k]])
+    sent(r.line_out.at[pl.ds(0, LINE - 1)], r.line_send)
 
 
 def layer_call(
@@ -919,13 +918,13 @@
         mixed_core_send=dma,
         mixed_core_recv=dma((2,)),
         mixed_pair_send=dma,
-        mixed_pair_recv=dma((MIXED_CUTS,)),
+        mixed_pair_recv=dma,
         share_send=dma,
         share_recv=dma((blocks,)),
         own_send=dma((2,)),
-        onward_send=dma((LINE,)),
+        onward_send=dma,
         along_recv=dma((LINE, parts)),
-        across_send=dma((LINE,)),
+        across_send=dma,
         across_recv=dma((LINE, parts)),
         partner_send=dma((LINE,)),
         partner_recv=dma((LINE, 2)),
@@ -933,13 +932,13 @@
         core_recv=dma((LINE,)),
         down_send=dma,
         down_recv=dma,
-        active_send=dma((LINE,)),
+        active_send=dma,
         active_recv=dma((LINE,)),
-        pair_send=dma((LINE,)),
+        pair_send=dma,
         pair_recv=dma((LINE, 2)),
-        side_send=dma((LINE,)),
+        side_send=dma,
         side_recv=dma((LINE, chunks)),
-        line_send=dma((LINE,)),
+        line_send=dma,
         line_recv=dma((2, LINE, chunks)),
         last_send=dma,
         last_recv=dma,

time: 71.6 us -> 71.2 us (level)
  no operation moved by 1% of the time
where the time goes in v4:
time: 71.2 us; the launch traced here: 71.1 us
  Pallas kernels  68.9 us (97%)
  local copies, waits for them, and re-layouts  1.5 us (2%)
    pallas_call x1, Pallas kernels, layer_call(): pl.pallas_call(layer_kernel, out_shape=(pltpu.VMEM((span, width), kept),...  68.9 us
    unnamed x2, local copies, waits for them, and re-layouts  1.5 us

profile of v4, /device:TPU:0, one launch (start us, length us, event | category | flops | bytes accessed | tf_op | source)
XLA Modules:
  0.0 71.1 jit_solution(11539820241272013240)
XLA Ops:
  0.6 68.9 %shard_map.131 = (bf16[64,4096]{1,0:T(8,128)(2,1)S(1)}, bf16[128,1024]{1,0:T(8,128)(2,1)S(1)}) custom-call(bf16[128,4096]{1,0:T(8,128)(2,1)} %refs_0_.1, f32[1,4096]{1,0:T(1,128)} %bitcast.9, s32[4,128]{1,0:T(4,128)} %bitcast.10, f32[4,128]{1,0:T(4,128)} %bitcast.11, bf16[256,512]{1,0:T(8,128)(2,1)} %refs_4_.1, bf16[256,128]{1,0:T(8,128)(2,1)} %refs_5_.1, ...), custom_call_target="tpu_custom_call" | custom-call | flops 8589934592 | bytes 8388608 | tf_op jit(solution)/shard_map/pallas_call | solution.py:946
  69.6 0.8 %copy.16 = bf16[64,4096]{1,0:T(8,128)(2,1)} copy(bf16[64,4096]{1,0:T(8,128)(2,1)S(1)} %get-tuple-element.2) | data formatting | bytes 1048576
  70.4 0.7 copy.17
